TPU v7x, 256 devices: a whole 4x4x8 slice. The times are simulated.
256 devices in a mesh: row: 32 (over z, y), col: 8 (over x, core).
Axes of the slice: x: 4, y: 4, z: 8, core: 2. Of those that a mesh axis runs over, the one named last changes fastest.
Arguments:
- tokens: bfloat16 [2, 65536, 1024], P(None, 'row'), may hold values from -6 to 6
- norm_gain: float32 [1024], replicated, may hold values from 0.1 to 1.9
- w_fourier_in: bfloat16 [1024, 512], P(None, 'col'), may hold values from -0.1875 to 0.1875
- w_gate: bfloat16 [1024, 1024], replicated, may hold values from -0.1875 to 0.1875
- w_spectrum: bfloat16 [512, 1024], replicated, may hold values from -0.25 to 0.25
- w_output: bfloat16 [1024, 1024], P(None, 'col'), may hold values from -0.375 to 0.375
Outputs:
- block_output: bfloat16 [2, 65536, 1024], P(None, 'row', 'col')
All inputs are finite; a program needn't handle non-finite values.
Results may differ from a plain program's by a relative error of at most 0.015.
Values may be sent and summed in bfloat16 or wider, within the bound.
A program may use at most 320 MiB of HBM per device.

v0:
```python
import jax
import jax.numpy as jnp
from jax import lax
from jax.sharding import PartitionSpec as P

GROUP_WIDTH = 64
FIRST_LEN = 256


norm_eps = 1e-06


def shortened(value):
    return jax.tree.map(lambda a: a.astype(jnp.bfloat16) if a.dtype == jnp.float32 else a, value)


def over_all(value, axis, dim, absorb, carry):
    whole = jax.tree.map(lambda part: lax.all_gather(part, axis, axis=dim, tiled=True), value)
    return absorb(carry, whole, jnp.int32(0))


def dft_tables(length_in, length_out, period):
    left_index = lax.broadcasted_iota(jnp.int32, (length_in, length_out), 0)
    right_index = lax.broadcasted_iota(jnp.int32, (length_in, length_out), 1)
    angles = (left_index * right_index % period).astype(jnp.float32) * (2.0 * jnp.pi / period)
    return (jnp.cos(angles), jnp.sin(angles))


def transform_first(cube, table):
    return jnp.einsum("cpq,pk->ckq", cube, table, precision=lax.Precision.HIGHEST)


def transform_second(cube, table):
    return jnp.einsum("ckq,qj->cjk", cube, table, precision=lax.Precision.HIGHEST)


def positional(real_part, imag_part):
    rows_count, seq_total = real_part.shape
    second_len = seq_total // FIRST_LEN
    cos_first, sin_first = dft_tables(FIRST_LEN, FIRST_LEN, FIRST_LEN)
    cos_twist, sin_twist = dft_tables(FIRST_LEN, second_len, seq_total)
    cos_second, sin_second = dft_tables(second_len, second_len, second_len)
    real_cube = real_part.reshape(rows_count, FIRST_LEN, second_len)
    imag_cube = imag_part.reshape(rows_count, FIRST_LEN, second_len)
    section_real = transform_first(real_cube, cos_first) + transform_first(imag_cube, sin_first)
    section_imag = transform_first(imag_cube, cos_first) - transform_first(real_cube, sin_first)
    twist_real = section_real * cos_twist + section_imag * sin_twist
    twist_imag = section_imag * cos_twist - section_real * sin_twist
    summed = transform_second(twist_real, cos_second) + transform_second(twist_imag, sin_second)
    norm_scale = 1.0 / jnp.sqrt(jnp.float32(seq_total * GROUP_WIDTH))
    return (summed.reshape(rows_count, seq_total) * norm_scale).astype(jnp.bfloat16)


def on_device(tokens, norm_gain, w_fourier_in, w_gate, w_spectrum, w_output):
    batches, seq_local, features = tokens.shape
    tokens_count = batches * seq_local
    widened = tokens.astype(jnp.float32)
    inverse = lax.rsqrt(jnp.mean(widened * widened, axis=-1, keepdims=True) + norm_eps)
    normed = (widened * inverse * norm_gain).astype(jnp.bfloat16).reshape(tokens_count, features)
    fourier_in = jnp.dot(normed, w_fourier_in, preferred_element_type=jnp.float32).astype(
        jnp.bfloat16
    )
    local_groups = w_fourier_in.shape[1] // GROUP_WIDTH
    grouped = fourier_in.astype(jnp.float32).reshape(batches, seq_local, local_groups, GROUP_WIDTH)
    cos_group, sin_group = dft_tables(GROUP_WIDTH, GROUP_WIDTH, GROUP_WIDTH)
    real_part = jnp.einsum(
        "btgn,nm->bgmt", grouped, cos_group, precision=lax.Precision.HIGHEST
    ).reshape(-1, seq_local)
    imag_part = -jnp.einsum(
        "btgn,nm->bgmt", grouped, sin_group, precision=lax.Precision.HIGHEST
    ).reshape(-1, seq_local)
    real_part = lax.all_to_all(
        shortened(real_part), "row", split_axis=0, concat_axis=1, tiled=True
    ).astype(real_part.dtype)
    imag_part = lax.all_to_all(
        shortened(imag_part), "row", split_axis=0, concat_axis=1, tiled=True
    ).astype(imag_part.dtype)
    spectrum = positional(real_part, imag_part)
    spectrum = lax.all_to_all(spectrum, "row", split_axis=1, concat_axis=0, tiled=True)
    spectrum = spectrum.reshape(batches, local_groups * GROUP_WIDTH, seq_local)
    spectrum = jnp.transpose(spectrum, (0, 2, 1)).reshape(tokens_count, local_groups * GROUP_WIDTH)

    def add_spectrum(running, portion, beginning):
        weight_rows = lax.dynamic_slice_in_dim(w_spectrum, beginning, portion.shape[1], 0)
        return running + jnp.dot(portion, weight_rows, preferred_element_type=jnp.float32)

    mixed_pre = over_all(
        spectrum, "col", 1, add_spectrum, jnp.zeros((tokens_count, features), jnp.float32)
    ).astype(jnp.bfloat16)
    gate_pre = jnp.dot(normed, w_gate, preferred_element_type=jnp.float32)
    mixed = (jax.nn.sigmoid(gate_pre) * mixed_pre.astype(jnp.float32)).astype(jnp.bfloat16)
    result = jnp.dot(mixed, w_output, preferred_element_type=jnp.float32)
    return result.astype(jnp.bfloat16).reshape(batches, seq_local, -1)


def solution(mesh):
    placed = (P(None, "row", None), P(), P(None, "col"), P(), P(), P(None, "col"))
    return jax.shard_map(
        on_device, mesh=mesh, in_specs=placed, out_specs=P(None, "row", "col"), check_vma=False
    )
```

profile of v0, /device:TPU:1, one launch (start us, length us, event | category | flops | bytes accessed | tf_op | source)
XLA Modules:
  0.0 175.4 jit_solution(16493660522271949661)
XLA Ops:
  6.5 0.0 copy-start
  6.5 0.0 copy-start.2
  6.5 0.0 copy-start.5
  6.5 5.2 %fusion = f32[2,2048]{1,0:T(2,128)S(1)} fusion(bf16[2,2048,1024]{2,1,0:T(8,128)(2,1)} %param.6), kind=kLoop, calls=%fused_computation.2 | loop fusion | flops 12578816 | bytes 8404992 | tf_op jit(solution)/shard_map/reduce_sum | solution.py:58
  11.8 0.6 copy-done.2
  12.5 0.0 copy-done.5
  12.5 2.2 %fusion.2 = bf16[2,2048,1024]{2,1,0:T(8,128)(2,1)S(1)} fusion(bf16[2,2048,1024]{2,1,0:T(8,128)(2,1)S(1)} %copy-done.2, f32[1024]{0:T(1024)S(1)} %copy-done.5, f32[2,2048]{1,0:T(2,128)S(1)} %add_rsqrt_fusion), kind=kLoop, calls=%fused_computation.4 | loop fusion | flops 16777216 | bytes 16797696 | tf_op jit(solution)/shard_map/convert_element_type | solution.py:59
  14.7 0.0 copy-start.1
  14.7 3.2 %copy-done.1 = bf16[2,2048,1024]{2,1,0:T(8,128)(2,1)} copy-done((bf16[2,2048,1024]{2,1,0:T(8,128)(2,1)}, bf16[2,2048,1024]{2,1,0:T(8,128)(2,1)S(1)}, u32[]{:S(2)}) %copy-start.1) | copy-done | bytes 8388632
  17.9 0.0 copy-done.4
  17.9 2.7 %convolution_convert_fusion = bf16[4096,64]{0,1:T(8,128)(2,1)S(1)} fusion(bf16[4096,1024]{1,0:T(8,128)(2,1)S(1)} %bitcast.69, bf16[1024,64]{0,1:T(8,128)(2,1)S(1)} %copy-done.4), kind=kOutput, calls=%fused_computation.8 | convolution fusion | flops 537133056 | bytes 9043968 | tf_op jit(solution)/shard_map/dot_general | solution.py:60
  20.5 0.7 fusion.7
  21.2 1.0 convert_element_type.107
  22.2 12.0 %all-to-all-start.1 = ((bf16[32,4,2048]{2,1,0:T(4,128)(2,1)}), bf16[32,4,2048]{2,1,0:T(4,128)(2,1)S(1)}, u32[]{:S(2)}, u32[]{:S(2)}) async-start(bf16[32,4,2048]{2,1,0:T(4,128)(2,1)} %convert_element_type.107), calls=%async_computation.1 | async-start | bytes 1048576 | tf_op jit(solution)/shard_map/all_to_all | solution.py:75
  34.3 1.5 fusion.6
  35.8 2.1 %convert_element_type.103 = bf16[32,4,2048]{2,1,0:T(4,128)(2,1)} reshape(bf16[2,1,64,2048]{3,2,0,1:T(8,128)(2,1)} %fusion.6) | data formatting | bytes 1048576 | tf_op jit(solution)/shard_map/convert_element_type | solution.py:14
  37.9 12.5 %all-to-all-done.1 = bf16[32,4,2048]{2,1,0:T(4,128)(2,1)S(1)} async-done(((bf16[32,4,2048]{2,1,0:T(4,128)(2,1)}), bf16[32,4,2048]{2,1,0:T(4,128)(2,1)S(1)}, u32[]{:S(2)}, u32[]{:S(2)}) %all-to-all-start.1) | async-done | bytes 524320 | tf_op jit(solution)/shard_map/all_to_all | solution.py:75
  50.3 5.7 %all-to-all-start = ((bf16[32,4,2048]{2,1,0:T(4,128)(2,1)}), bf16[32,4,2048]{2,1,0:T(4,128)(2,1)}, u32[]{:S(2)}, u32[]{:S(2)}) async-start(bf16[32,4,2048]{2,1,0:T(4,128)(2,1)} %convert_element_type.103), calls=%async_computation | async-start | bytes 1048576 | tf_op jit(solution)/shard_map/all_to_all | solution.py:72
  56.0 0.2 all-gather.2.cloned.1.call-start
  56.3 1.0 fusion.48
  57.2 0.1 copy.17
  57.4 1.0 fusion.47
  58.3 0.8 copy.18
  59.2 0.3 copy.16
  59.5 0.2 reshape.92
  59.7 11.3 %all-to-all-done = bf16[32,4,2048]{2,1,0:T(4,128)(2,1)} async-done(((bf16[32,4,2048]{2,1,0:T(4,128)(2,1)}), bf16[32,4,2048]{2,1,0:T(4,128)(2,1)}, u32[]{:S(2)}, u32[]{:S(2)}) %all-to-all-start) | async-done | bytes 524320 | tf_op jit(solution)/shard_map/all_to_all | solution.py:72
  71.0 2.1 %copy.14 = bf16[4,32,2048]{2,1,0:T(8,128)(2,1)} copy(bf16[4,32,2048]{2,0,1:T(4,128)(2,1)} %bitcast.5) | data formatting | bytes 1048576 | tf_op jit(solution)/shard_map/all_to_all | solution.py:72
  73.2 1.3 reshape.91
  74.5 0.0 copy-start.3
  74.5 1.5 fusion.38
  76.0 1.5 fusion.36
  77.5 1.6 convolution_add_fusion
  79.1 1.6 convolution_subtract_fusion
  80.7 0.0 copy-done.3
  80.7 2.1 %fusion.12 = f32[256,4,256]{2,0,1:T(8,128)S(1)} fusion(f32[256,4,256]{2,0,1:T(8,128)S(1)} %convolution_subtract_fusion, f32[256,4,256]{2,0,1:T(8,128)S(1)} %convolution_add_fusion, f32[256,256]{1,0:T(8,128)S(1)} %copy-done.3, f32[256,256]{1,0:T(8,128)S(1)} %copy.17), kind=kOutput, calls=%fused_computation.21 | convolution fusion | flops 807010304 | bytes 3670016 | tf_op jit(solution)/shard_map/ckq,qj->cjk/dot_general | solution.py:34
  82.8 2.4 %fusion.10 = bf16[4,256,256]{2,1,0:T(8,128)(2,1)S(1)} fusion(f32[256,4,256]{2,0,1:T(8,128)S(1)} %fusion.12, f32[256,4,256]{2,0,1:T(8,128)S(1)} %convolution_add_fusion, f32[256,4,256]{2,0,1:T(8,128)S(1)} %convolution_subtract_fusion, f32[256,256]{1,0:T(8,128)S(1)} %copy-done.3, f32[256,256]{1,0:T(8,128)S(1)} %copy.17), kind=kOutput, calls=%fused_computation.19 | convolution fusion | flops 807796736 | bytes 4194304 | tf_op jit(solution)/shard_map/ckq,qj->cjk/dot_general | solution.py:34
  85.2 0.2 convert_element_type.111
  85.5 0.4 copy.19
  85.9 21.5 %all_to_all.39 = bf16[4,32,2048]{2,0,1:T(4,128)(2,1)S(1)} all-to-all(bf16[4,32,2048]{2,0,1:T(4,128)(2,1)S(1)} %copy.19), channel_id=1, replica_groups=mesh['row'=32,'col'=8] {'row'}, dimensions={1} | all-to-all | bytes 1048576 | tf_op jit(solution)/shard_map/all_to_all | solution.py:79
  107.4 0.1 reshape.93
  107.6 0.8 copy.22
  108.4 0.0 all-gather.2.cloned.1.call-update
  108.4 0.0 copy-start.6
  108.4 33.1 %all-gather.2.cloned.1.call-done = bf16[4096,512]{0,1:T(8,128)(2,1)} async-done(((bf16[4096,64]{0,1:T(8,128)(2,1)}), bf16[4096,512]{0,1:T(8,128)(2,1)}) %all-gather.2.cloned.1.call-update) | async-done | bytes 4194320 | tf_op jit(solution)/shard_map/all_gather | solution.py:18
  141.5 10.3 %fusion.102 = bf16[4096,1024]{1,0:T(8,128)(2,1)} fusion(bf16[4096,512]{0,1:T(8,128)(2,1)} %all-gather.2.cloned.1.call-done, bf16[512,1024]{1,0:T(8,128)(2,1)} %param.10), kind=kOutput, calls=%fused_computation.113 | convolution fusion | flops 4294967296 | bytes 13631488 | tf_op jit(solution)/shard_map/dot_general | solution.py:85
  151.8 0.0 copy-done
  151.8 0.0 copy-done.6
  151.8 16.7 %fusion.4 = bf16[4096,128]{1,0:T(8,128)(2,1)} fusion(bf16[1024,128]{1,0:T(8,128)(2,1)S(1)} %copy-done.6, bf16[4096,1024]{1,0:T(8,128)(2,1)} %bitcast.70, bf16[1024,1024]{1,0:T(8,128)(2,1)S(1)} %copy-done, bf16[4096,1024]{1,0:T(8,128)(2,1)} %fusion.102), kind=kOutput, calls=%fused_computation.7 | convolution fusion | flops 9689366528 | bytes 20185088 | tf_op jit(solution)/shard_map/dot_general | solution.py:92
  (2 shorter events, 0.0 us)
Async XLA Ops:
  6.5 145.3 %copy-start = (bf16[1024,1024]{1,0:T(8,128)(2,1)S(1)}, bf16[1024,1024]{1,0:T(8,128)(2,1)}, u32[]{:S(2)}) copy-start(bf16[1024,1024]{1,0:T(8,128)(2,1)} %param.9) | copy-start | bytes 6291460
  6.5 5.9 %copy-start.2 = (bf16[2,2048,1024]{2,1,0:T(8,128)(2,1)S(1)}, bf16[2,2048,1024]{2,1,0:T(8,128)(2,1)}, u32[]{:S(2)}) copy-start(bf16[2,2048,1024]{2,1,0:T(8,128)(2,1)} %param.6) | copy-start | bytes 25165828
  6.5 5.9 %copy-start.5 = (f32[1024]{0:T(1024)S(1)}, f32[1024]{0:T(1024)}, u32[]{:S(2)}) copy-start(f32[1024]{0:T(1024)} %param.7) | copy-start | bytes 12292
  12.5 5.4 %copy-start.4 = (bf16[1024,64]{0,1:T(8,128)(2,1)S(1)}, bf16[1024,64]{0,1:T(8,128)(2,1)}, u32[]{:S(2)}) copy-start(bf16[1024,64]{0,1:T(8,128)(2,1)} %param.8) | copy-start | bytes 393220
  14.7 3.2 %copy-start.1 = (bf16[2,2048,1024]{2,1,0:T(8,128)(2,1)}, bf16[2,2048,1024]{2,1,0:T(8,128)(2,1)S(1)}, u32[]{:S(2)}) copy-start(bf16[2,2048,1024]{2,1,0:T(8,128)(2,1)S(1)} %fusion.2) | copy-start | bytes 25165828
  22.2 28.1 %all-to-all-start.1 = ((bf16[32,4,2048]{2,1,0:T(4,128)(2,1)}), bf16[32,4,2048]{2,1,0:T(4,128)(2,1)S(1)}, u32[]{:S(2)}, u32[]{:S(2)}) async-start(bf16[32,4,2048]{2,1,0:T(4,128)(2,1)} %convert_element_type.107), calls=%async_computation.1 | async-start | bytes 1048576 | tf_op jit(solution)/shard_map/all_to_all | solution.py:75
  50.3 20.7 %all-to-all-start = ((bf16[32,4,2048]{2,1,0:T(4,128)(2,1)}), bf16[32,4,2048]{2,1,0:T(4,128)(2,1)}, u32[]{:S(2)}, u32[]{:S(2)}) async-start(bf16[32,4,2048]{2,1,0:T(4,128)(2,1)} %convert_element_type.103), calls=%async_computation | async-start | bytes 1048576 | tf_op jit(solution)/shard_map/all_to_all | solution.py:72
  56.0 85.5 %all-gather.2.cloned.1.call-start = ((), (), s32[]{:S(2)}) async-start(), calls=%async_computation.3 | async-start | bytes 4718592 | tf_op jit(solution)/shard_map/all_gather | solution.py:18
  74.5 6.2 %copy-start.3 = (f32[256,256]{1,0:T(8,128)S(1)}, f32[256,256]{1,0:T(8,128)}, u32[]{:S(2)}) copy-start(f32[256,256]{1,0:T(8,128)} %copy.18) | copy-start | bytes 786436
  108.4 43.4 %copy-start.6 = (bf16[1024,128]{1,0:T(8,128)(2,1)S(1)}, bf16[1024,128]{1,0:T(8,128)(2,1)}, u32[]{:S(2)}) copy-start(bf16[1024,128]{1,0:T(8,128)(2,1)} %param.11) | copy-start | bytes 786436
Sparse Core Ops, SparseCore 0:
  108.5 32.9 all-gather.1
where the time goes:
time: 176 us; the launch traced here: 175 us
  waiting for transfers between devices  56.9 us (32%)
  matrix products  42.6 us (24%)
  blocking collectives  21.5 us (12%)
  starting transfers between devices  17.9 us (10%)
  between operations  13.6 us (8%)
  local copies, waits for them, and re-layouts  13.4 us (8%)
  other arithmetic  9.39 us (5%)
    all_gather x1, waiting for transfers between devices, over_all(): lax.all_gather(part, axis, axis=dim, tiled=True)  33.1 us
    all_to_all x1, blocking collectives, on_device(): lax.all_to_all(spectrum, 'row', split_axis=1, concat_axis=0, tiled=True)  21.5 us
    dot_general x1, matrix products, on_device(): result = jnp.dot(mixed, w_output, preferred_element_type=jnp.float32)  16.7 us
    all_to_all x1, waiting for transfers between devices, on_device(): lax.all_to_all(shortened(imag_part), 'row', split_axis=0, concat_axis=1,...  12.5 us
    all_to_all x1, starting transfers between devices, on_device(): lax.all_to_all(shortened(imag_part), 'row', split_axis=0, concat_axis=1,...  12 us
    all_to_all x1, waiting for transfers between devices, on_device(): lax.all_to_all(shortened(real_part), 'row', split_axis=0, concat_axis=1,...  11.3 us
    dot_general x1, matrix products, add_spectrum(): jnp.dot(portion, weight_rows, preferred_element_type=jnp.float32)  10.3 us
    dot_general x4, matrix products, transform_first(): jnp.einsum('cpq,pk->ckq', cube, table, precision=lax.Precision.HIGHEST)  6.18 us
  transfers between devices with their start and end apart: 3, of which 3 were waited for; matrix products, arithmetic and copies ran while one was open for 4% of the time, Pallas kernels for 0%

commit v1 on v0

v1 whole, which is shorter than its diff:
```python
import numpy as np
import jax
import jax.numpy as jnp
from jax import lax
from jax.experimental import pallas as pl
from jax.experimental.pallas import tpu as pltpu
from jax.sharding import PartitionSpec as P

MESH = pl.DeviceIdType.MESH
ROWS, COLS = 32, 8
SEQS, LOCAL, D = 2, 2048, 1024
TILE = 256
TILES = LOCAL // TILE
SEQ = ROWS * LOCAL
WIDTH = 64
CHANNELS = COLS * WIDTH
OUT = D // COLS
EPS = 1e-6
F32, BF16 = jnp.float32, jnp.bfloat16


def partner_channel(r, second):
    if r == 0:
        return 32 * second
    return WIDTH - r if second else r


def tables():
    n = np.arange(WIDTH)[:, None]
    analysis = np.zeros((2 * WIDTH, WIDTH))
    for r in range(ROWS):
        analysis[2 * r] = np.cos(2 * np.pi * n[:, 0] * r / WIDTH)
        analysis[2 * r + 1] = np.sin(2 * np.pi * n[:, 0] * r / WIDTH) if r else np.cos(np.pi * n[:, 0])
    a = np.arange(256)[:, None]
    p = np.arange(256)[None, :]
    turn = 2 * np.pi * (a * p % 256) / 256
    first = np.zeros((ROWS, 2, TILES, 4, 256))
    for e in range(2):
        first[:, e, :, 2 * e] = np.cos(turn).reshape(ROWS, TILES, 256)
        first[:, e, :, 2 * e + 1] = -np.sin(turn).reshape(ROWS, TILES, 256)
    first = first.reshape(2 * ROWS * TILES, 4 * 256)
    twist = 2 * np.pi * (a * p) / SEQ
    twist = np.concatenate([np.cos(twist), -np.sin(twist)], axis=1)
    second = np.concatenate([np.cos(turn), np.sin(turn)], axis=1) / np.sqrt(SEQ * WIDTH)
    select = np.zeros((CHANNELS, CHANNELS))
    for r in range(ROWS):
        for ch in range(2):
            for c in range(COLS):
                select[r * 16 + ch * 8 + c, c * WIDTH + partner_channel(r, ch)] = 1.0
    return (
        jnp.asarray(analysis, BF16),
        jnp.asarray(first, BF16),
        jnp.asarray(twist, F32),
        jnp.asarray(second, BF16),
        jnp.asarray(select, BF16),
    )


def dot(x, y, dims=((1,), (0,))):
    return lax.dot_general(x, y, (dims, ((), ())), preferred_element_type=F32)


def kernel(
    tokens, gain, w_in, w_gate, w_spec, w_out, analysis, first, twist, second, select,
    out,
    tok, gain_v, w_in_v, wc, w_gate_v, w_spec_v, w_map, w_out_v,
    analysis_v, first_v, twist_v, second_v, select_v,
    turned, send1, recv1, mid, both, sendx, recvx, wide, send2, recv2, sig, result,
    tok_sem, load_sem, s1, r1, sx, rx, s2, r2, so, ro, own_o, sw, rw, sf, rf,
):
    row, col = lax.axis_index("row"), lax.axis_index("col")
    chip, core = col // 2, col % 2

    barrier = pltpu.get_barrier_semaphore()

    def greet_row(d, _):
        pl.semaphore_signal(barrier, inc=1, device_id=((row + d) % ROWS, col), device_id_type=MESH)
        return 0

    def greet_col(d, _):
        pl.semaphore_signal(barrier, inc=1, device_id=(row, (col + d) % COLS), device_id_type=MESH)
        return 0

    lax.fori_loop(1, ROWS, greet_row, 0)
    lax.fori_loop(1, COLS, greet_col, 0)

    def cols_of(c):
        return pl.ds(pl.multiple_of(c * OUT, OUT), OUT)

    loads = [
        pltpu.make_async_copy(src, dst, load_sem.at[i])
        for i, (src, dst) in enumerate(
            [
                (analysis, analysis_v), (w_in, w_in_v), (gain, gain_v),
                (first, first_v), (twist, twist_v), (second, second_v),
                (w_gate, w_gate_v), (w_out, w_out_v.at[:, cols_of(col)]),
                (w_spec, w_spec_v), (select, select_v),
            ]
        )
    ]

    def tile_copy(b, j):
        return pltpu.make_async_copy(
            tokens.at[b, pl.ds(pl.multiple_of(j * TILE, TILE), TILE)], tok.at[b, j], tok_sem.at[b, j]
        )

    for i in range(3):
        loads[i].start()
    for b in range(SEQS):
        for j in range(TILES):
            tile_copy(b, j).start()
    for i in range(3, 10):
        loads[i].start()

    for i in range(3):
        loads[i].wait()
    folded = dot(analysis_v[...], w_in_v[...], ((1,), (1,))) * gain_v[...]
    wc[...] = jnp.transpose(folded).astype(BF16)

    def rows16(r):
        return pl.ds(pl.multiple_of(16 * r, 16), 16)

    def strided(ref, lo, hi, count, stride):
        halves = [
            jnp.concatenate([ref[h, pl.ds(at, count, stride), :] for at in (lo, hi)], axis=0) for h in range(2)
        ]
        return jnp.concatenate(halves, axis=1).astype(BF16)

    def project(b):
        def tile(j, _):
            tile_copy(b, j).wait()
            t = tok[b, j]
            wide_t = t.astype(F32)
            inverse = lax.rsqrt(jnp.sum(wide_t * wide_t, axis=1, keepdims=True) * (1.0 / D) + EPS)
            y = dot(t, wc[...]) * inverse
            flipped = jnp.transpose(y)[:WIDTH]
            for h in range(2):
                turned[h, pl.ds(pl.multiple_of(j * WIDTH, WIDTH), WIDTH), :] = flipped[:, 128 * h : 128 * (h + 1)]
            return 0

        lax.fori_loop(0, TILES, tile, 0)

        def pick(r, _):
            send1[b, rows16(r), :] = strided(turned, 2 * r, 2 * r + 1, TILES, WIDTH)
            return 0

        lax.fori_loop(0, ROWS, pick, 0)

    def row_copy(src, dst, ssem, rsem, b, peer):
        return pltpu.make_async_remote_copy(
            src_ref=src.at[b, rows16(peer)], dst_ref=dst.at[b, rows16(row)],
            send_sem=ssem.at[b], recv_sem=rsem.at[b], device_id=(peer, col), device_id_type=MESH,
        )

    def row_send(src, dst, ssem, rsem, b):
        def one(d, _):
            row_copy(src, dst, ssem, rsem, b, (row + d) % ROWS).start()
            return 0

        lax.fori_loop(1, ROWS, one, 0)
        dst[b, rows16(row), :] = src[b, rows16(row), :]

    def wait_bytes(ref, sem):
        pltpu.make_async_copy(ref, ref, sem).wait()

    most = pl.ds(0, 16 * (ROWS - 1))

    def col_send(b):
        def one(d, _):
            peer = (col + d) % COLS
            pltpu.make_async_remote_copy(
                src_ref=sendx.at[b, peer], dst_ref=recvx.at[b, col],
                send_sem=sx.at[b], recv_sem=rx.at[b], device_id=(row, peer), device_id_type=MESH,
            ).start()
            return 0

        lax.fori_loop(1, COLS, one, 0)
        recvx[b, col] = sendx[b, col]

    def fourier(b):
        wait_bytes(recv1.at[b, most], r1.at[b])
        y = dot(recv1[b], first_v[...], ((0,), (0,)))
        tr, ti = twist_v[:, :256], twist_v[:, 256:]
        ar, ai, br, bi = (y[:, 256 * i : 256 * (i + 1)] for i in range(4))
        pa, qa = ar * tr - ai * ti, ar * ti + ai * tr
        pb, qb = br * tr - bi * ti, br * ti + bi * tr
        lone = row == 0
        both[:256, :256] = pa.astype(BF16)
        both[256:, :256] = qa.astype(BF16)
        both[:256, 256:] = jnp.where(lone, pb, -qb).astype(BF16)
        both[256:, 256:] = jnp.where(lone, qb, pb).astype(BF16)
        d = dot(second_v[...], both[...])
        da, db = d[:, :256], d[:, 256:]
        made = (jnp.where(lone, da, da - db), jnp.where(lone, db, da + db))
        for ch in range(2):
            for h in range(2):
                mid[h, 256 * ch : 256 * (ch + 1)] = made[ch][:, 128 * h : 128 * (h + 1)]

        def pick(c, _):
            sendx[b, c] = strided(mid, c, 256 + c, ROWS, COLS)
            return 0

        lax.fori_loop(0, COLS, pick, 0)

    def regroup(b):
        wait_bytes(recvx.at[b, pl.ds(0, COLS - 1)], rx.at[b])

        def widen(c, _):
            block = recvx[b, c].astype(F32)
            for h in range(2):
                wide[h, pl.ds(pl.multiple_of(c * WIDTH, WIDTH), WIDTH), :] = block[:, 128 * h : 128 * (h + 1)]
            return 0

        lax.fori_loop(0, COLS, widen, 0)

        def pick(r, _):
            send2[b, rows16(r), :] = strided(wide, r, ROWS + r, COLS, WIDTH)
            return 0

        lax.fori_loop(0, ROWS, pick, 0)

    def gates(b):
        t = tok[b, col].astype(F32)
        inverse = lax.rsqrt(jnp.sum(t * t, axis=1, keepdims=True) * (1.0 / D) + EPS)
        normed = (t * inverse * gain_v[...]).astype(BF16)
        sig[b] = jax.nn.sigmoid(dot(normed, w_gate_v[...]))

    def share_out(d):
        peer = ((chip + d) % 4) * 2 + core
        return pltpu.make_async_remote_copy(
            src_ref=w_out_v.at[:, cols_of(col)], dst_ref=w_out_v.at[:, cols_of(col)],
            send_sem=sw, recv_sem=rw, device_id=(row, peer), device_id_type=MESH,
        )

    def pass_out(d):
        held = cols_of(((chip + d) % 4) * 2 + core)
        return pltpu.make_async_remote_copy(
            src_ref=w_out_v.at[:, held], dst_ref=w_out_v.at[:, held],
            send_sem=sf, recv_sem=rf, device_id=(row, chip * 2 + 1 - core), device_id_type=MESH,
        )

    def finish(b):
        wait_bytes(recv2.at[b, most], r2.at[b])
        pre = dot(recv2[b], w_map[...], ((0,), (0,))).astype(BF16).astype(F32)
        mixed = (sig[b] * pre).astype(BF16)
        result[b] = dot(mixed, w_out_v[...]).astype(BF16)
        place = pl.ds(pl.multiple_of(col * TILE, TILE), TILE)

        def one(d, _):
            peer = (col + d) % COLS
            pltpu.make_async_remote_copy(
                src_ref=result.at[b, :, cols_of(peer)], dst_ref=out.at[b, place],
                send_sem=so.at[b], recv_sem=ro.at[b], device_id=(row, peer), device_id_type=MESH,
            ).start()
            return 0

        lax.fori_loop(1, COLS, one, 0)
        pltpu.make_async_copy(result.at[b, :, cols_of(col)], out.at[b, place], own_o.at[b]).start()

    project(0)
    pl.semaphore_wait(barrier, ROWS - 1 + COLS - 1)
    row_send(send1, recv1, s1, r1, 0)
    project(1)
    row_send(send1, recv1, s1, r1, 1)

    loads[7].wait()
    for d in range(1, 4):
        share_out(d).start()
    pass_out(0).start()

    loads[6].wait()
    gates(0)
    gates(1)
    loads[8].wait()
    loads[9].wait()
    w_map[...] = dot(select_v[...], w_spec_v[...]).astype(BF16)

    for i in range(3, 6):
        loads[i].wait()
    fourier(0)
    col_send(0)
    regroup(0)
    row_send(send2, recv2, s2, r2, 0)
    fourier(1)
    col_send(1)

    shard = w_out_v.at[:, pl.ds(0, 3 * OUT)]
    wait_bytes(shard, rw)
    for d in range(1, 4):
        pass_out(d).start()

    regroup(1)
    row_send(send2, recv2, s2, r2, 1)
    wait_bytes(w_out_v.at[:, pl.ds(0, 4 * OUT)], rf)
    finish(0)
    finish(1)

    wait_bytes(shard, sw)
    wait_bytes(w_out_v.at[:, pl.ds(0, 4 * OUT)], sf)
    for b in range(SEQS):
        wait_bytes(send1.at[b, most], s1.at[b])
        wait_bytes(sendx.at[b, pl.ds(0, COLS - 1)], sx.at[b])
        wait_bytes(send2.at[b, most], s2.at[b])
        wait_bytes(result.at[b, :, pl.ds(0, (COLS - 1) * OUT)], so.at[b])
        wait_bytes(out.at[b, pl.ds(0, (COLS - 1) * TILE)], ro.at[b])
        wait_bytes(result.at[b, :, pl.ds(0, OUT)], own_o.at[b])


def on_device(tokens, norm_gain, w_fourier_in, w_gate, w_spectrum, w_output):
    dma = pltpu.SemaphoreType.DMA
    pair = dma((SEQS,))
    scratch = [
        pltpu.VMEM((SEQS, TILES, TILE, D), BF16),
        pltpu.VMEM((1, D), F32),
        pltpu.VMEM((D, WIDTH), BF16),
        pltpu.VMEM((D, 2 * WIDTH), BF16),
        pltpu.VMEM((D, D), BF16),
        pltpu.VMEM((CHANNELS, D), BF16),
        pltpu.VMEM((CHANNELS, D), BF16),
        pltpu.VMEM((D, D), BF16),
        pltpu.VMEM((2 * WIDTH, WIDTH), BF16),
        pltpu.VMEM((512, 1024), BF16),
        pltpu.VMEM((256, 512), F32),
        pltpu.VMEM((256, 512), BF16),
        pltpu.VMEM((CHANNELS, CHANNELS), BF16),
        pltpu.VMEM((2, TILES * WIDTH, 128), F32),
        pltpu.VMEM((SEQS, 16 * ROWS, 256), BF16),
        pltpu.VMEM((SEQS, 16 * ROWS, 256), BF16),
        pltpu.VMEM((2, 512, 128), F32),
        pltpu.VMEM((512, 512), BF16),
        pltpu.VMEM((SEQS, COLS, WIDTH, 256), BF16),
        pltpu.VMEM((SEQS, COLS, WIDTH, 256), BF16),
        pltpu.VMEM((2, COLS * WIDTH, 128), F32),
        pltpu.VMEM((SEQS, 16 * ROWS, 256), BF16),
        pltpu.VMEM((SEQS, 16 * ROWS, 256), BF16),
        pltpu.VMEM((SEQS, TILE, D), F32),
        pltpu.VMEM((SEQS, TILE, D), BF16),
        dma((SEQS, TILES)), dma((10,)),
        pair, pair, pair, pair, pair, pair, pair, pair, pair,
        dma, dma, dma, dma,
    ]
    anywhere = pl.BlockSpec(memory_space=pl.ANY)
    return pl.pallas_call(
        kernel,
        out_shape=jax.ShapeDtypeStruct((SEQS, LOCAL, OUT), BF16),
        in_specs=[anywhere] * 11,
        out_specs=anywhere,
        scratch_shapes=scratch,
        compiler_params=pltpu.CompilerParams(
            collective_id=0, has_side_effects=True, vmem_limit_bytes=56 * 1024 * 1024
        ),
        name="fourier_mix",
    )(tokens, norm_gain.reshape(1, D), w_fourier_in, w_gate, w_spectrum, w_output, *tables())


def solution(mesh):
    placed = (P(None, "row", None), P(), P(None, "col"), P(), P(), P(None, "col"))
    return jax.shard_map(
        on_device, mesh=mesh, in_specs=placed, out_specs=P(None, "row", "col"), check_vma=False
    )
```

time: 176 us -> 67.7 us (0.38)
  Pallas kernels: 0 us -> 63.6 us
  waiting for transfers between devices: 56.9 us -> 0 us
  matrix products: 42.6 us -> 0 us
  blocking collectives: 21.5 us -> 0 us
  starting transfers between devices: 17.9 us -> 0 us
  between operations: 13.6 us -> 0.01 us
  other arithmetic: 9.39 us -> 0 us
  local copies, waits for them, and re-layouts: 13.4 us -> 4.01 us
    pallas_call x0 -> x1, Pallas kernels: none -> 63.6 us  [on_device(): pl.pallas_call(kernel, out_shape=jax.ShapeDtypeStruct((SEQS, LOCAL, OUT),...]
    dot_general x11 -> x0, matrix products: 42.6 us -> none  [the longest x1 16.7 us: on_device(): result = jnp.dot(mixed, w_output, preferred_element_type=jnp.float32)]
    all_gather x1 -> x0, waiting for transfers between devices: 33.1 us -> none  [over_all(): lax.all_gather(part, axis, axis=dim, tiled=True)]
    all_to_all x2 -> x0, waiting for transfers between devices: 23.8 us -> none  [the longest x1 12.5 us: on_device(): lax.all_to_all(shortened(imag_part), 'row', split_axis=0, concat_axis=1,...]
    all_to_all x1 -> x0, blocking collectives: 21.5 us -> none  [on_device(): lax.all_to_all(spectrum, 'row', split_axis=1, concat_axis=0, tiled=True)]
    all_to_all x2 -> x0, starting transfers between devices: 17.7 us -> none  [the longest x1 12 us: on_device(): lax.all_to_all(shortened(imag_part), 'row', split_axis=0, concat_axis=1,...]
    reduce_sum x1 -> x0, other arithmetic: 5.25 us -> none  [on_device(): jnp.mean(widened * widened, axis=-1, keepdims=True) + norm_eps]
    convert_element_type x4 -> x0, local copies, waits for them, and re-layouts: 3.69 us -> none  [the longest x2 3.04 us: shortened(): a.astype(jnp.bfloat16)]
  transfers between devices with their start and end apart: 3 -> 0, of which waited for: 3 -> 0; matrix products, arithmetic and copies ran while one was open for 4% -> 0% of each run, Pallas kernels for 0% -> 0%
where the time goes in v1:
time: 67.7 us; the launch traced here: 67.6 us
  Pallas kernels  63.6 us (94%)
  local copies, waits for them, and re-layouts  4.01 us (6%)
    pallas_call x1, Pallas kernels, on_device(): pl.pallas_call(kernel, out_shape=jax.ShapeDtypeStruct((SEQS, LOCAL, OUT),...  63.6 us
    unnamed x2, local copies, waits for them, and re-layouts  4.01 us

profile of v1, /device:TPU:1, one launch (start us, length us, event | category | flops | bytes accessed | tf_op | source)
XLA Modules:
  0.0 67.6 jit_solution(16528868519338521389)
XLA Ops:
  0.0 1.7 %copy.12.w_in = bf16[1024,64]{1,0:T(8,128)(2,1)} copy(bf16[1024,64]{0,1:T(8,128)(2,1)} %param.13) | data formatting | bytes 262144 | tf_op args[2]
  1.7 63.6 %fourier_mix.1 = bf16[2,2048,128]{2,1,0:T(8,128)(2,1)} custom-call(bf16[2,2048,1024]{2,1,0:T(8,128)(2,1)} %tokens.1, f32[1,1024]{1,0:T(1,128)} %bitcast.1, bf16[1024,64]{1,0:T(8,128)(2,1)} %copy.12.w_in, bf16[1024,1024]{1,0:T(8,128)(2,1)} %w_gate.1, bf16[512,1024]{1,0:T(8,128)(2,1)} %w_spec.1, bf16[1024,128]{1,0:T(8,128)(2,1)} %w_out.1, ...), custom_call_target="tpu_custom_call" | custom-call | tf_op jit(solution)/shard_map/fourier_mix/pallas_call | solution.py:343
  65.3 2.3 %copy.14 = bf16[2,2048,128]{2,1,0:T(8,128)(2,1)} copy(bf16[2,2048,128]{2,1,0:T(8,128)(2,1)} %fourier_mix.1) | data formatting | bytes 2097152

commit v2 on v1

--- a/solution.py
+++ b/solution.py
@@ -66,7 +66,7 @@
     tok, gain_v, w_in_v, wc, w_gate_v, w_spec_v, w_map, w_out_v,
     analysis_v, first_v, twist_v, second_v, select_v,
     turned, send1, recv1, mid, both, sendx, recvx, wide, send2, recv2, sig, result,
-    tok_sem, load_sem, s1, r1, sx, rx, s2, r2, so, ro, own_o, sw, rw, sf, rf,
+    tok_sem, load_sem, s1, r1, sx, rx, s2, r2, so, ro, own_o, swo, rwo, swn, rwn, swy, rwy, sf, rf,
 ):
     row, col = lax.axis_index("row"), lax.axis_index("col")
     chip, core = col // 2, col % 2
@@ -114,7 +114,7 @@
 
     for i in range(3):
         loads[i].wait()
-    folded = dot(analysis_v[...], w_in_v[...], ((1,), (1,))) * gain_v[...]
+    folded = dot(analysis_v[...], w_in_v[...]) * gain_v[...]
     wc[...] = jnp.transpose(folded).astype(BF16)
 
     def rows16(r):
@@ -146,19 +146,20 @@
 
         lax.fori_loop(0, ROWS, pick, 0)
 
-    def row_copy(src, dst, ssem, rsem, b, peer):
-        return pltpu.make_async_remote_copy(
-            src_ref=src.at[b, rows16(peer)], dst_ref=dst.at[b, rows16(row)],
-            send_sem=ssem.at[b], recv_sem=rsem.at[b], device_id=(peer, col), device_id_type=MESH,
-        )
-
-    def row_send(src, dst, ssem, rsem, b):
-        def one(d, _):
-            row_copy(src, dst, ssem, rsem, b, (row + d) % ROWS).start()
-            return 0
-
-        lax.fori_loop(1, ROWS, one, 0)
-        dst[b, rows16(row), :] = src[b, rows16(row), :]
+    def row_send(src, dst, ssem, rsem, lanes):
+        def one(i, _):
+            k, l = i // 4, i % 4
+            dz = 4 + (k + 1) // 2 * (1 - 2 * (k % 2))
+            dy = 2 + (l + 1) // 2 * (1 - 2 * (l % 2))
+            peer = (row // 4 + dz) % 8 * 4 + (row % 4 + dy) % 4
+            pltpu.make_async_remote_copy(
+                src_ref=src.at[rows16(peer), lanes], dst_ref=dst.at[rows16(row), lanes],
+                send_sem=ssem, recv_sem=rsem, device_id=(peer, col), device_id_type=MESH,
+            ).start()
+            return 0
+
+        lax.fori_loop(0, ROWS - 1, one, 0)
+        dst[rows16(row), lanes] = src[rows16(row), lanes]
 
     def wait_bytes(ref, sem):
         pltpu.make_async_copy(ref, ref, sem).wait()
@@ -178,7 +179,6 @@
         recvx[b, col] = sendx[b, col]
 
     def fourier(b):
-        wait_bytes(recv1.at[b, most], r1.at[b])
         y = dot(recv1[b], first_v[...], ((0,), (0,)))
         tr, ti = twist_v[:, :256], twist_v[:, 256:]
         ar, ai, br, bi = (y[:, 256 * i : 256 * (i + 1)] for i in range(4))
@@ -203,8 +203,6 @@
         lax.fori_loop(0, COLS, pick, 0)
 
     def regroup(b):
-        wait_bytes(recvx.at[b, pl.ds(0, COLS - 1)], rx.at[b])
-
         def widen(c, _):
             block = recvx[b, c].astype(F32)
             for h in range(2):
@@ -225,94 +223,116 @@
         normed = (t * inverse * gain_v[...]).astype(BF16)
         sig[b] = jax.nn.sigmoid(dot(normed, w_gate_v[...]))
 
-    def share_out(d):
-        peer = ((chip + d) % 4) * 2 + core
+    quarter = pl.ds(pl.multiple_of(row % 4 * 256, 256), 256)
+
+    def shard_of(d):
+        return cols_of((chip + d) % 4 * 2 + core)
+
+    def share_out(rows, d, ssem, rsem, peer):
         return pltpu.make_async_remote_copy(
-            src_ref=w_out_v.at[:, cols_of(col)], dst_ref=w_out_v.at[:, cols_of(col)],
-            send_sem=sw, recv_sem=rw, device_id=(row, peer), device_id_type=MESH,
+            src_ref=w_out_v.at[rows, shard_of(d)], dst_ref=w_out_v.at[rows, shard_of(d)],
+            send_sem=ssem, recv_sem=rsem, device_id=peer, device_id_type=MESH,
         )
 
-    def pass_out(d):
-        held = cols_of(((chip + d) % 4) * 2 + core)
-        return pltpu.make_async_remote_copy(
-            src_ref=w_out_v.at[:, held], dst_ref=w_out_v.at[:, held],
-            send_sem=sf, recv_sem=rf, device_id=(row, chip * 2 + 1 - core), device_id_type=MESH,
-        )
-
-    def finish(b):
-        wait_bytes(recv2.at[b, most], r2.at[b])
-        pre = dot(recv2[b], w_map[...], ((0,), (0,))).astype(BF16).astype(F32)
-        mixed = (sig[b] * pre).astype(BF16)
-        result[b] = dot(mixed, w_out_v[...]).astype(BF16)
-        place = pl.ds(pl.multiple_of(col * TILE, TILE), TILE)
+    def at_chip(d):
+        return (row, (chip + d) % 4 * 2 + core)
+
+    every = pl.ds(0, D)
+    other_core = (row, chip * 2 + 1 - core)
+
+    def finish(b, h):
+        lanes = pl.ds(128 * h, 128)
+        pre = dot(recv2[b, :, lanes], w_map[...], ((0,), (0,))).astype(BF16).astype(F32)
+        mixed = (sig[b, lanes] * pre).astype(BF16)
+        result[b, lanes] = dot(mixed, w_out_v[...]).astype(BF16)
+        place = pl.ds(pl.multiple_of(col * TILE + 128 * h, 128), 128)
 
         def one(d, _):
             peer = (col + d) % COLS
             pltpu.make_async_remote_copy(
-                src_ref=result.at[b, :, cols_of(peer)], dst_ref=out.at[b, place],
-                send_sem=so.at[b], recv_sem=ro.at[b], device_id=(row, peer), device_id_type=MESH,
+                src_ref=result.at[b, lanes, cols_of(peer)], dst_ref=out.at[b, place],
+                send_sem=so.at[b, h], recv_sem=ro.at[b, h], device_id=(row, peer), device_id_type=MESH,
             ).start()
             return 0
 
         lax.fori_loop(1, COLS, one, 0)
-        pltpu.make_async_copy(result.at[b, :, cols_of(col)], out.at[b, place], own_o.at[b]).start()
+        pltpu.make_async_copy(result.at[b, lanes, cols_of(col)], out.at[b, place], own_o.at[b, h]).start()
+
+    whole = pl.ds(0, 256)
+
+    def forward(b):
+        row_send(send1.at[b], recv1.at[b], s1.at[b], r1.at[b], whole)
+
+    def back(b):
+        for h in range(2):
+            row_send(send2.at[b], recv2.at[b], s2.at[b, h], r2.at[b, h], pl.ds(128 * h, 128))
 
     project(0)
     pl.semaphore_wait(barrier, ROWS - 1 + COLS - 1)
-    row_send(send1, recv1, s1, r1, 0)
+    forward(0)
+    loads[7].wait()
+    share_out(quarter, 0, swo, rwo, at_chip(2)).start()
+    share_out(every, 0, swn, rwn, at_chip(1)).start()
+    share_out(every, 0, swn, rwn, at_chip(3)).start()
+    share_out(every, 0, sf, rf, other_core).start()
     project(1)
-    row_send(send1, recv1, s1, r1, 1)
-
-    loads[7].wait()
+    wait_bytes(w_out_v.at[pl.ds(0, 256), pl.ds(0, OUT)], rwo)
     for d in range(1, 4):
-        share_out(d).start()
-    pass_out(0).start()
-
+        share_out(quarter, 2, swy, rwy, (row // 4 * 4 + (row % 4 + d) % 4, col)).start()
     loads[6].wait()
     gates(0)
-    gates(1)
     loads[8].wait()
     loads[9].wait()
     w_map[...] = dot(select_v[...], w_spec_v[...]).astype(BF16)
-
     for i in range(3, 6):
         loads[i].wait()
+
+    wait_bytes(recv1.at[0, most], r1.at[0])
+    forward(1)
     fourier(0)
     col_send(0)
+    gates(1)
+    wait_bytes(recvx.at[0, pl.ds(0, COLS - 1)], rx.at[0])
     regroup(0)
-    row_send(send2, recv2, s2, r2, 0)
+    back(0)
+    wait_bytes(w_out_v.at[:, pl.ds(0, 2 * OUT)], rwn)
+    wait_bytes(w_out_v.at[pl.ds(0, 768), pl.ds(0, OUT)], rwy)
+    for d in range(1, 4):
+        share_out(every, d, sf, rf, other_core).start()
+    wait_bytes(recv1.at[1, most], r1.at[1])
     fourier(1)
     col_send(1)
-
-    shard = w_out_v.at[:, pl.ds(0, 3 * OUT)]
-    wait_bytes(shard, rw)
-    for d in range(1, 4):
-        pass_out(d).start()
-
+    wait_bytes(recvx.at[1, pl.ds(0, COLS - 1)], rx.at[1])
     regroup(1)
-    row_send(send2, recv2, s2, r2, 1)
+    back(1)
     wait_bytes(w_out_v.at[:, pl.ds(0, 4 * OUT)], rf)
-    finish(0)
-    finish(1)
-
-    wait_bytes(shard, sw)
+    for b in range(SEQS):
+        for h in range(2):
+            wait_bytes(recv2.at[b, most, pl.ds(128 * h, 128)], r2.at[b, h])
+            finish(b, h)
+
+    wait_bytes(w_out_v.at[pl.ds(0, 256), pl.ds(0, OUT)], swo)
+    wait_bytes(w_out_v.at[:, pl.ds(0, 2 * OUT)], swn)
+    wait_bytes(w_out_v.at[pl.ds(0, 768), pl.ds(0, OUT)], swy)
     wait_bytes(w_out_v.at[:, pl.ds(0, 4 * OUT)], sf)
     for b in range(SEQS):
         wait_bytes(send1.at[b, most], s1.at[b])
         wait_bytes(sendx.at[b, pl.ds(0, COLS - 1)], sx.at[b])
-        wait_bytes(send2.at[b, most], s2.at[b])
-        wait_bytes(result.at[b, :, pl.ds(0, (COLS - 1) * OUT)], so.at[b])
-        wait_bytes(out.at[b, pl.ds(0, (COLS - 1) * TILE)], ro.at[b])
-        wait_bytes(result.at[b, :, pl.ds(0, OUT)], own_o.at[b])
+        for h in range(2):
+            lanes = pl.ds(128 * h, 128)
+            wait_bytes(send2.at[b, most, lanes], s2.at[b, h])
+            wait_bytes(result.at[b, lanes, pl.ds(0, (COLS - 1) * OUT)], so.at[b, h])
+            wait_bytes(out.at[b, pl.ds(0, (COLS - 1) * 128)], ro.at[b, h])
+            wait_bytes(result.at[b, lanes, pl.ds(0, OUT)], own_o.at[b, h])
 
 
 def on_device(tokens, norm_gain, w_fourier_in, w_gate, w_spectrum, w_output):
     dma = pltpu.SemaphoreType.DMA
-    pair = dma((SEQS,))
+    pair, halves = dma((SEQS,)), dma((SEQS, 2))
     scratch = [
         pltpu.VMEM((SEQS, TILES, TILE, D), BF16),
         pltpu.VMEM((1, D), F32),
-        pltpu.VMEM((D, WIDTH), BF16),
+        pltpu.VMEM((WIDTH, D), BF16),
         pltpu.VMEM((D, 2 * WIDTH), BF16),
         pltpu.VMEM((D, D), BF16),
         pltpu.VMEM((CHANNELS, D), BF16),
@@ -336,8 +356,8 @@
         pltpu.VMEM((SEQS, TILE, D), F32),
         pltpu.VMEM((SEQS, TILE, D), BF16),
         dma((SEQS, TILES)), dma((10,)),
-        pair, pair, pair, pair, pair, pair, pair, pair, pair,
-        dma, dma, dma, dma,
+        pair, pair, pair, pair, halves, halves, halves, halves, halves,
+        dma, dma, dma, dma, dma, dma, dma, dma,
     ]
     anywhere = pl.BlockSpec(memory_space=pl.ANY)
     return pl.pallas_call(
@@ -350,7 +370,7 @@
             collective_id=0, has_side_effects=True, vmem_limit_bytes=56 * 1024 * 1024
         ),
         name="fourier_mix",
-    )(tokens, norm_gain.reshape(1, D), w_fourier_in, w_gate, w_spectrum, w_output, *tables())
+    )(tokens, norm_gain.reshape(1, D), w_fourier_in.T, w_gate, w_spectrum, w_output, *tables())
 
 
 def solution(mesh):

time: 67.7 us -> 59.6 us (0.88)
  Pallas kernels: 63.6 us -> 57.2 us
  local copies, waits for them, and re-layouts: 4.01 us -> 2.26 us
    pallas_call x1, Pallas kernels: 63.6 us -> 57.2 us  [on_device(): pl.pallas_call(kernel, out_shape=jax.ShapeDtypeStruct((SEQS, LOCAL, OUT),...]
    unnamed x2 -> x1, local copies, waits for them, and re-layouts: 4.01 us -> 2.26 us
where the time goes in v2:
time: 59.6 us; the launch traced here: 59.5 us
  Pallas kernels  57.2 us (96%)
  local copies, waits for them, and re-layouts  2.26 us (4%)
    pallas_call x1, Pallas kernels, on_device(): pl.pallas_call(kernel, out_shape=jax.ShapeDtypeStruct((SEQS, LOCAL, OUT),...  57.2 us
    unnamed x1, local copies, waits for them, and re-layouts  2.26 us

profile of v2, /device:TPU:1, one launch (start us, length us, event | category | flops | bytes accessed | tf_op | source)
XLA Modules:
  0.0 59.5 jit_solution(13159712655810005745)
XLA Ops:
  0.0 57.2 %fourier_mix.1 = bf16[2,2048,128]{2,1,0:T(8,128)(2,1)} custom-call(bf16[2,2048,1024]{2,1,0:T(8,128)(2,1)} %tokens.1, f32[1,1024]{1,0:T(1,128)} %bitcast.3, bf16[64,1024]{1,0:T(8,128)(2,1)} %bitcast.2, bf16[1024,1024]{1,0:T(8,128)(2,1)} %w_gate.1, bf16[512,1024]{1,0:T(8,128)(2,1)} %w_spec.1, bf16[1024,128]{1,0:T(8,128)(2,1)} %w_out.1, ...), custom_call_target="tpu_custom_call" | custom-call | tf_op jit(solution)/shard_map/fourier_mix/pallas_call | solution.py:363
  57.2 2.3 %copy.13 = bf16[2,2048,128]{2,1,0:T(8,128)(2,1)} copy(bf16[2,2048,128]{2,1,0:T(8,128)(2,1)} %fourier_mix.1) | data formatting | bytes 2097152

commit v3 on v2

--- a/solution.py
+++ b/solution.py
@@ -38,9 +38,10 @@
     for e in range(2):
         first[:, e, :, 2 * e] = np.cos(turn).reshape(ROWS, TILES, 256)
         first[:, e, :, 2 * e + 1] = -np.sin(turn).reshape(ROWS, TILES, 256)
-    first = first.reshape(2 * ROWS * TILES, 4 * 256)
+    first = first.reshape(2 * ROWS * TILES, 4, 2, 128).transpose(2, 0, 1, 3).reshape(2, 2 * ROWS * TILES, 512)
     twist = 2 * np.pi * (a * p) / SEQ
-    twist = np.concatenate([np.cos(twist), -np.sin(twist)], axis=1)
+    twist = np.stack([np.cos(twist), -np.sin(twist)], axis=1).reshape(256, 2, 2, 128)
+    twist = twist.transpose(2, 0, 1, 3).reshape(2, 256, 256)
     second = np.concatenate([np.cos(turn), np.sin(turn)], axis=1) / np.sqrt(SEQ * WIDTH)
     select = np.zeros((CHANNELS, CHANNELS))
     for r in range(ROWS):
@@ -120,11 +121,9 @@
     def rows16(r):
         return pl.ds(pl.multiple_of(16 * r, 16), 16)
 
-    def strided(ref, lo, hi, count, stride):
-        halves = [
-            jnp.concatenate([ref[h, pl.ds(at, count, stride), :] for at in (lo, hi)], axis=0) for h in range(2)
-        ]
-        return jnp.concatenate(halves, axis=1).astype(BF16)
+    def strided(ref, h, lo, hi, count, stride):
+        rows = [ref[h, pl.ds(at, count, stride), :] for at in (lo, hi)]
+        return jnp.concatenate(rows, axis=0).astype(BF16)
 
     def project(b):
         def tile(j, _):
@@ -140,82 +139,81 @@
 
         lax.fori_loop(0, TILES, tile, 0)
 
-        def pick(r, _):
-            send1[b, rows16(r), :] = strided(turned, 2 * r, 2 * r + 1, TILES, WIDTH)
+        def pick(i, _):
+            for u in range(4):
+                r = 4 * i + u
+                for h in range(2):
+                    lanes = slice(128 * h, 128 * (h + 1))
+                    send1[b, rows16(r), lanes] = strided(turned, h, 2 * r, 2 * r + 1, TILES, WIDTH)
             return 0
 
-        lax.fori_loop(0, ROWS, pick, 0)
-
-    def row_send(src, dst, ssem, rsem, lanes):
-        def one(i, _):
-            k, l = i // 4, i % 4
-            dz = 4 + (k + 1) // 2 * (1 - 2 * (k % 2))
-            dy = 2 + (l + 1) // 2 * (1 - 2 * (l % 2))
-            peer = (row // 4 + dz) % 8 * 4 + (row % 4 + dy) % 4
+        lax.fori_loop(0, ROWS // 4, pick, 0)
+
+    peers_z = [((row // 4 + dz) % 8) * 4 for dz in range(8)]
+    peers_y = [(row % 4 + dy) % 4 for dy in range(4)]
+    far_first = sorted(
+        ((dz, dy) for dz in range(8) for dy in range(4) if dz or dy),
+        key=lambda o: -(min(o[0], 8 - o[0]) + min(o[1], 4 - o[1])),
+    )
+
+    def row_send(src, dst, ssem, rsem):
+        mine = rows16(row)
+        for dz, dy in far_first:
+            peer = peers_z[dz] + peers_y[dy]
             pltpu.make_async_remote_copy(
-                src_ref=src.at[rows16(peer), lanes], dst_ref=dst.at[rows16(row), lanes],
+                src_ref=src.at[rows16(peer)], dst_ref=dst.at[mine],
                 send_sem=ssem, recv_sem=rsem, device_id=(peer, col), device_id_type=MESH,
             ).start()
-            return 0
-
-        lax.fori_loop(0, ROWS - 1, one, 0)
-        dst[rows16(row), lanes] = src[rows16(row), lanes]
+        dst[mine, :] = src[mine, :]
 
     def wait_bytes(ref, sem):
         pltpu.make_async_copy(ref, ref, sem).wait()
 
     most = pl.ds(0, 16 * (ROWS - 1))
-
-    def col_send(b):
-        def one(d, _):
-            peer = (col + d) % COLS
+    peers_c = [(col + d) % COLS for d in range(COLS)]
+    col_order = (4, 5, 3, 2, 6, 7, 1)
+
+    def col_send(b, h):
+        for d in col_order:
+            peer = peers_c[d]
             pltpu.make_async_remote_copy(
-                src_ref=sendx.at[b, peer], dst_ref=recvx.at[b, col],
-                send_sem=sx.at[b], recv_sem=rx.at[b], device_id=(row, peer), device_id_type=MESH,
+                src_ref=sendx.at[b, h, peer], dst_ref=recvx.at[b, h, col],
+                send_sem=sx.at[b, h], recv_sem=rx.at[b, h], device_id=(row, peer), device_id_type=MESH,
             ).start()
+        recvx[b, h, col] = sendx[b, h, col]
+
+    def fourier(b):
+        lone = row == 0
+        across = jnp.transpose(recv1[b])
+        for h in range(2):
+            y = dot(across, first_v[h])
+            tr, ti = twist_v[h, :, :128], twist_v[h, :, 128:]
+            ar, ai, br, bi = (y[:, 128 * i : 128 * (i + 1)] for i in range(4))
+            pa, qa = ar * tr - ai * ti, ar * ti + ai * tr
+            pb, qb = br * tr - bi * ti, br * ti + bi * tr
+            both[h, :256, :128] = pa.astype(BF16)
+            both[h, 256:, :128] = qa.astype(BF16)
+            both[h, :256, 128:] = jnp.where(lone, pb, -qb).astype(BF16)
+            both[h, 256:, 128:] = jnp.where(lone, qb, pb).astype(BF16)
+            d = dot(second_v[...], both[h])
+            da, db = d[:, :128], d[:, 128:]
+            mid[h, :256] = jnp.where(lone, da, da - db)
+            mid[h, 256:] = jnp.where(lone, db, da + db)
+            for c in range(COLS):
+                sendx[b, h, c] = strided(mid, h, c, 256 + c, ROWS, COLS)
+            col_send(b, h)
+
+    def regroup(b, h):
+        for c in range(COLS):
+            wide[h, c * WIDTH : (c + 1) * WIDTH, :] = recvx[b, h, c].astype(F32)
+
+        def pick(i, _):
+            for u in range(4):
+                r = 4 * i + u
+                send2[b, h, rows16(r), :] = strided(wide, h, r, ROWS + r, COLS, WIDTH)
             return 0
 
-        lax.fori_loop(1, COLS, one, 0)
-        recvx[b, col] = sendx[b, col]
-
-    def fourier(b):
-        y = dot(recv1[b], first_v[...], ((0,), (0,)))
-        tr, ti = twist_v[:, :256], twist_v[:, 256:]
-        ar, ai, br, bi = (y[:, 256 * i : 256 * (i + 1)] for i in range(4))
-        pa, qa = ar * tr - ai * ti, ar * ti + ai * tr
-        pb, qb = br * tr - bi * ti, br * ti + bi * tr
-        lone = row == 0
-        both[:256, :256] = pa.astype(BF16)
-        both[256:, :256] = qa.astype(BF16)
-        both[:256, 256:] = jnp.where(lone, pb, -qb).astype(BF16)
-        both[256:, 256:] = jnp.where(lone, qb, pb).astype(BF16)
-        d = dot(second_v[...], both[...])
-        da, db = d[:, :256], d[:, 256:]
-        made = (jnp.where(lone, da, da - db), jnp.where(lone, db, da + db))
-        for ch in range(2):
-            for h in range(2):
-                mid[h, 256 * ch : 256 * (ch + 1)] = made[ch][:, 128 * h : 128 * (h + 1)]
-
-        def pick(c, _):
-            sendx[b, c] = strided(mid, c, 256 + c, ROWS, COLS)
-            return 0
-
-        lax.fori_loop(0, COLS, pick, 0)
-
-    def regroup(b):
-        def widen(c, _):
-            block = recvx[b, c].astype(F32)
-            for h in range(2):
-                wide[h, pl.ds(pl.multiple_of(c * WIDTH, WIDTH), WIDTH), :] = block[:, 128 * h : 128 * (h + 1)]
-            return 0
-
-        lax.fori_loop(0, COLS, widen, 0)
-
-        def pick(r, _):
-            send2[b, rows16(r), :] = strided(wide, r, ROWS + r, COLS, WIDTH)
-            return 0
-
-        lax.fori_loop(0, ROWS, pick, 0)
+        lax.fori_loop(0, ROWS // 4, pick, 0)
 
     def gates(b):
         t = tok[b, col].astype(F32)
@@ -242,30 +240,26 @@
 
     def finish(b, h):
         lanes = pl.ds(128 * h, 128)
-        pre = dot(recv2[b, :, lanes], w_map[...], ((0,), (0,))).astype(BF16).astype(F32)
+        pre = dot(recv2[b, h], w_map[...], ((0,), (0,))).astype(BF16).astype(F32)
         mixed = (sig[b, lanes] * pre).astype(BF16)
         result[b, lanes] = dot(mixed, w_out_v[...]).astype(BF16)
         place = pl.ds(pl.multiple_of(col * TILE + 128 * h, 128), 128)
 
-        def one(d, _):
-            peer = (col + d) % COLS
+        for d in col_order:
+            peer = peers_c[d]
             pltpu.make_async_remote_copy(
                 src_ref=result.at[b, lanes, cols_of(peer)], dst_ref=out.at[b, place],
                 send_sem=so.at[b, h], recv_sem=ro.at[b, h], device_id=(row, peer), device_id_type=MESH,
             ).start()
-            return 0
-
-        lax.fori_loop(1, COLS, one, 0)
         pltpu.make_async_copy(result.at[b, lanes, cols_of(col)], out.at[b, place], own_o.at[b, h]).start()
 
-    whole = pl.ds(0, 256)
-
     def forward(b):
-        row_send(send1.at[b], recv1.at[b], s1.at[b], r1.at[b], whole)
-
-    def back(b):
-        for h in range(2):
-            row_send(send2.at[b], recv2.at[b], s2.at[b, h], r2.at[b, h], pl.ds(128 * h, 128))
+        row_send(send1.at[b], recv1.at[b], s1.at[b], r1.at[b])
+
+    def back(b, h):
+        wait_bytes(recvx.at[b, h, pl.ds(0, COLS - 1)], rx.at[b, h])
+        regroup(b, h)
+        row_send(send2.at[b, h], recv2.at[b, h], s2.at[b, h], r2.at[b, h])
 
     project(0)
     pl.semaphore_wait(barrier, ROWS - 1 + COLS - 1)
@@ -276,39 +270,35 @@
     share_out(every, 0, swn, rwn, at_chip(3)).start()
     share_out(every, 0, sf, rf, other_core).start()
     project(1)
-    wait_bytes(w_out_v.at[pl.ds(0, 256), pl.ds(0, OUT)], rwo)
-    for d in range(1, 4):
-        share_out(quarter, 2, swy, rwy, (row // 4 * 4 + (row % 4 + d) % 4, col)).start()
     loads[6].wait()
     gates(0)
     loads[8].wait()
     loads[9].wait()
     w_map[...] = dot(select_v[...], w_spec_v[...]).astype(BF16)
+    forward(1)
+    gates(1)
+    wait_bytes(w_out_v.at[pl.ds(0, 256), pl.ds(0, OUT)], rwo)
+    for d in range(1, 4):
+        share_out(quarter, 2, swy, rwy, (row // 4 * 4 + (row % 4 + d) % 4, col)).start()
     for i in range(3, 6):
         loads[i].wait()
 
     wait_bytes(recv1.at[0, most], r1.at[0])
-    forward(1)
     fourier(0)
-    col_send(0)
-    gates(1)
-    wait_bytes(recvx.at[0, pl.ds(0, COLS - 1)], rx.at[0])
-    regroup(0)
-    back(0)
+    back(0, 0)
+    back(0, 1)
+    wait_bytes(recv1.at[1, most], r1.at[1])
+    fourier(1)
     wait_bytes(w_out_v.at[:, pl.ds(0, 2 * OUT)], rwn)
     wait_bytes(w_out_v.at[pl.ds(0, 768), pl.ds(0, OUT)], rwy)
     for d in range(1, 4):
         share_out(every, d, sf, rf, other_core).start()
-    wait_bytes(recv1.at[1, most], r1.at[1])
-    fourier(1)
-    col_send(1)
-    wait_bytes(recvx.at[1, pl.ds(0, COLS - 1)], rx.at[1])
-    regroup(1)
-    back(1)
+    back(1, 0)
+    back(1, 1)
     wait_bytes(w_out_v.at[:, pl.ds(0, 4 * OUT)], rf)
     for b in range(SEQS):
         for h in range(2):
-            wait_bytes(recv2.at[b, most, pl.ds(128 * h, 128)], r2.at[b, h])
+            wait_bytes(recv2.at[b, h, most], r2.at[b, h])
             finish(b, h)
 
     wait_bytes(w_out_v.at[pl.ds(0, 256), pl.ds(0, OUT)], swo)
@@ -317,10 +307,10 @@
     wait_bytes(w_out_v.at[:, pl.ds(0, 4 * OUT)], sf)
     for b in range(SEQS):
         wait_bytes(send1.at[b, most], s1.at[b])
-        wait_bytes(sendx.at[b, pl.ds(0, COLS - 1)], sx.at[b])
         for h in range(2):
             lanes = pl.ds(128 * h, 128)
-            wait_bytes(send2.at[b, most, lanes], s2.at[b, h])
+            wait_bytes(sendx.at[b, h, pl.ds(0, COLS - 1)], sx.at[b, h])
+            wait_bytes(send2.at[b, h, most], s2.at[b, h])
             wait_bytes(result.at[b, lanes, pl.ds(0, (COLS - 1) * OUT)], so.at[b, h])
             wait_bytes(out.at[b, pl.ds(0, (COLS - 1) * 128)], ro.at[b, h])
             wait_bytes(result.at[b, lanes, pl.ds(0, OUT)], own_o.at[b, h])
@@ -339,24 +329,24 @@
         pltpu.VMEM((CHANNELS, D), BF16),
         pltpu.VMEM((D, D), BF16),
         pltpu.VMEM((2 * WIDTH, WIDTH), BF16),
-        pltpu.VMEM((512, 1024), BF16),
-        pltpu.VMEM((256, 512), F32),
+        pltpu.VMEM((2, 512, 512), BF16),
+        pltpu.VMEM((2, 256, 256), F32),
         pltpu.VMEM((256, 512), BF16),
         pltpu.VMEM((CHANNELS, CHANNELS), BF16),
         pltpu.VMEM((2, TILES * WIDTH, 128), F32),
         pltpu.VMEM((SEQS, 16 * ROWS, 256), BF16),
         pltpu.VMEM((SEQS, 16 * ROWS, 256), BF16),
         pltpu.VMEM((2, 512, 128), F32),
-        pltpu.VMEM((512, 512), BF16),
-        pltpu.VMEM((SEQS, COLS, WIDTH, 256), BF16),
-        pltpu.VMEM((SEQS, COLS, WIDTH, 256), BF16),
+        pltpu.VMEM((2, 512, 256), BF16),
+        pltpu.VMEM((SEQS, 2, COLS, WIDTH, 128), BF16),
+        pltpu.VMEM((SEQS, 2, COLS, WIDTH, 128), BF16),
         pltpu.VMEM((2, COLS * WIDTH, 128), F32),
-        pltpu.VMEM((SEQS, 16 * ROWS, 256), BF16),
-        pltpu.VMEM((SEQS, 16 * ROWS, 256), BF16),
+        pltpu.VMEM((SEQS, 2, 16 * ROWS, 128), BF16),
+        pltpu.VMEM((SEQS, 2, 16 * ROWS, 128), BF16),
         pltpu.VMEM((SEQS, TILE, D), F32),
         pltpu.VMEM((SEQS, TILE, D), BF16),
         dma((SEQS, TILES)), dma((10,)),
-        pair, pair, pair, pair, halves, halves, halves, halves, halves,
+        pair, pair, halves, halves, halves, halves, halves, halves, halves,
         dma, dma, dma, dma, dma, dma, dma, dma,
     ]
     anywhere = pl.BlockSpec(memory_space=pl.ANY)

time: 59.6 us -> 50.8 us (0.85)
  Pallas kernels: 57.2 us -> 48.4 us
    pallas_call x1, Pallas kernels: 57.2 us -> 48.4 us  [on_device(): pl.pallas_call(kernel, out_shape=jax.ShapeDtypeStruct((SEQS, LOCAL, OUT),...]
where the time goes in v3:
time: 50.8 us; the launch traced here: 50.6 us
  Pallas kernels  48.4 us (95%)
  local copies, waits for them, and re-layouts  2.26 us (4%)
    pallas_call x1, Pallas kernels, on_device(): pl.pallas_call(kernel, out_shape=jax.ShapeDtypeStruct((SEQS, LOCAL, OUT),...  48.4 us
    unnamed x1, local copies, waits for them, and re-layouts  2.26 us

profile of v3, /device:TPU:1, one launch (start us, length us, event | category | flops | bytes accessed | tf_op | source)
XLA Modules:
  0.0 50.6 jit_solution(11562622128871478686)
XLA Ops:
  0.0 48.4 %fourier_mix.1 = bf16[2,2048,128]{2,1,0:T(8,128)(2,1)} custom-call(bf16[2,2048,1024]{2,1,0:T(8,128)(2,1)} %tokens.1, f32[1,1024]{1,0:T(1,128)} %bitcast.3, bf16[64,1024]{1,0:T(8,128)(2,1)} %bitcast.2, bf16[1024,1024]{1,0:T(8,128)(2,1)} %w_gate.1, bf16[512,1024]{1,0:T(8,128)(2,1)} %w_spec.1, bf16[1024,128]{1,0:T(8,128)(2,1)} %w_out.1, ...), custom_call_target="tpu_custom_call" | custom-call | tf_op jit(solution)/shard_map/fourier_mix/pallas_call | solution.py:353
  48.4 2.3 %copy.13 = bf16[2,2048,128]{2,1,0:T(8,128)(2,1)} copy(bf16[2,2048,128]{2,1,0:T(8,128)(2,1)} %fourier_mix.1) | data formatting | bytes 2097152

commit v4 on v3

--- a/solution.py
+++ b/solution.py
@@ -352,7 +352,7 @@
     anywhere = pl.BlockSpec(memory_space=pl.ANY)
     return pl.pallas_call(
         kernel,
-        out_shape=jax.ShapeDtypeStruct((SEQS, LOCAL, OUT), BF16),
+        out_shape=pltpu.VMEM((SEQS, LOCAL, OUT), BF16),
         in_specs=[anywhere] * 11,
         out_specs=anywhere,
         scratch_shapes=scratch,

time: 50.8 us -> 49.2 us (0.969)
  local copies, waits for them, and re-layouts: 2.26 us -> 0.97 us
    unnamed x1, local copies, waits for them, and re-layouts: 2.26 us -> 0.97 us
where the time goes in v4:
time: 49.2 us; the launch traced here: 49.1 us
  Pallas kernels  48.1 us (98%)
  local copies, waits for them, and re-layouts  0.97 us (2%)
    pallas_call x1, Pallas kernels, on_device(): pl.pallas_call(kernel, out_shape=pltpu.VMEM((SEQS, LOCAL, OUT), BF16), in...  48.1 us

profile of v4, /device:TPU:1, one launch (start us, length us, event | category | flops | bytes accessed | tf_op | source)
XLA Modules:
  0.0 49.1 jit_solution(4880133804469185292)
XLA Ops:
  0.0 48.1 %fourier_mix.1 = bf16[2,2048,128]{2,1,0:T(8,128)(2,1)S(1)} custom-call(bf16[2,2048,1024]{2,1,0:T(8,128)(2,1)} %tokens.1, f32[1,1024]{1,0:T(1,128)} %bitcast.3, bf16[64,1024]{1,0:T(8,128)(2,1)} %bitcast.2, bf16[1024,1024]{1,0:T(8,128)(2,1)} %w_gate.1, bf16[512,1024]{1,0:T(8,128)(2,1)} %w_spec.1, bf16[1024,128]{1,0:T(8,128)(2,1)} %w_out.1, ...), custom_call_target="tpu_custom_call" | custom-call | tf_op jit(solution)/shard_map/fourier_mix/pallas_call | solution.py:353
  48.1 1.0 %copy.13 = bf16[2,2048,128]{2,1,0:T(8,128)(2,1)} copy(bf16[2,2048,128]{2,1,0:T(8,128)(2,1)S(1)} %fourier_mix.1) | data formatting | bytes 2097152

commit v5 on v4

--- a/solution.py
+++ b/solution.py
@@ -11,6 +11,7 @@
 SEQS, LOCAL, D = 2, 2048, 1024
 TILE = 256
 TILES = LOCAL // TILE
+STEP = 2
 SEQ = ROWS * LOCAL
 WIDTH = 64
 CHANNELS = COLS * WIDTH
@@ -49,7 +50,7 @@
             for c in range(COLS):
                 select[r * 16 + ch * 8 + c, c * WIDTH + partner_channel(r, ch)] = 1.0
     return (
-        jnp.asarray(analysis, BF16),
+        jnp.asarray(analysis.T, BF16),
         jnp.asarray(first, BF16),
         jnp.asarray(twist, F32),
         jnp.asarray(second, BF16),
@@ -71,19 +72,6 @@
 ):
     row, col = lax.axis_index("row"), lax.axis_index("col")
     chip, core = col // 2, col % 2
-
-    barrier = pltpu.get_barrier_semaphore()
-
-    def greet_row(d, _):
-        pl.semaphore_signal(barrier, inc=1, device_id=((row + d) % ROWS, col), device_id_type=MESH)
-        return 0
-
-    def greet_col(d, _):
-        pl.semaphore_signal(barrier, inc=1, device_id=(row, (col + d) % COLS), device_id_type=MESH)
-        return 0
-
-    lax.fori_loop(1, ROWS, greet_row, 0)
-    lax.fori_loop(1, COLS, greet_col, 0)
 
     def cols_of(c):
         return pl.ds(pl.multiple_of(c * OUT, OUT), OUT)
@@ -107,6 +95,21 @@
 
     for i in range(3):
         loads[i].start()
+
+    peers_z = [((row // 4 + dz) % 8) * 4 for dz in range(8)]
+    peers_y = [(row % 4 + dy) % 4 for dy in range(4)]
+    peers_c = [(col + d) % COLS for d in range(COLS)]
+    far_first = sorted(
+        ((dz, dy) for dz in range(8) for dy in range(4) if dz or dy),
+        key=lambda o: -(min(o[0], 8 - o[0]) + min(o[1], 4 - o[1])),
+    )
+
+    barrier = pltpu.get_barrier_semaphore()
+    for dz, dy in far_first:
+        pl.semaphore_signal(barrier, inc=1, device_id=(peers_z[dz] + peers_y[dy], col), device_id_type=MESH)
+    for d in range(1, COLS):
+        pl.semaphore_signal(barrier, inc=1, device_id=(row, peers_c[d]), device_id_type=MESH)
+
     for b in range(SEQS):
         for j in range(TILES):
             tile_copy(b, j).start()
@@ -115,8 +118,8 @@
 
     for i in range(3):
         loads[i].wait()
-    folded = dot(analysis_v[...], w_in_v[...]) * gain_v[...]
-    wc[...] = jnp.transpose(folded).astype(BF16)
+    scaled = (w_in_v[...].astype(F32) * gain_v[...]).astype(BF16)
+    wc[...] = dot(scaled, analysis_v[...], ((0,), (0,))).astype(BF16)
 
     def rows16(r):
         return pl.ds(pl.multiple_of(16 * r, 16), 16)
@@ -126,35 +129,30 @@
         return jnp.concatenate(rows, axis=0).astype(BF16)
 
     def project(b):
-        def tile(j, _):
-            tile_copy(b, j).wait()
-            t = tok[b, j]
-            wide_t = t.astype(F32)
-            inverse = lax.rsqrt(jnp.sum(wide_t * wide_t, axis=1, keepdims=True) * (1.0 / D) + EPS)
-            y = dot(t, wc[...]) * inverse
-            flipped = jnp.transpose(y)[:WIDTH]
-            for h in range(2):
-                turned[h, pl.ds(pl.multiple_of(j * WIDTH, WIDTH), WIDTH), :] = flipped[:, 128 * h : 128 * (h + 1)]
+        def tiles(i, _):
+            for u in range(STEP):
+                tile_copy(b, STEP * i + u).wait()
+            for u in range(STEP):
+                j = STEP * i + u
+                t = tok[b, j]
+                wide_t = t.astype(F32)
+                inverse = lax.rsqrt(jnp.sum(wide_t * wide_t, axis=1, keepdims=True) * (1.0 / D) + EPS)
+                flipped = jnp.transpose(dot(t, wc[...]) * inverse)[:WIDTH]
+                for h in range(2):
+                    turned[h, pl.ds(pl.multiple_of(j * WIDTH, WIDTH), WIDTH), :] = flipped[:, 128 * h : 128 * (h + 1)]
             return 0
 
-        lax.fori_loop(0, TILES, tile, 0)
+        lax.fori_loop(0, TILES // STEP, tiles, 0)
 
         def pick(i, _):
-            for u in range(4):
-                r = 4 * i + u
+            for u in range(8):
+                r = 8 * i + u
                 for h in range(2):
                     lanes = slice(128 * h, 128 * (h + 1))
                     send1[b, rows16(r), lanes] = strided(turned, h, 2 * r, 2 * r + 1, TILES, WIDTH)
             return 0
 
-        lax.fori_loop(0, ROWS // 4, pick, 0)
-
-    peers_z = [((row // 4 + dz) % 8) * 4 for dz in range(8)]
-    peers_y = [(row % 4 + dy) % 4 for dy in range(4)]
-    far_first = sorted(
-        ((dz, dy) for dz in range(8) for dy in range(4) if dz or dy),
-        key=lambda o: -(min(o[0], 8 - o[0]) + min(o[1], 4 - o[1])),
-    )
+        lax.fori_loop(0, ROWS // 8, pick, 0)
 
     def row_send(src, dst, ssem, rsem):
         mine = rows16(row)
@@ -170,7 +168,6 @@
         pltpu.make_async_copy(ref, ref, sem).wait()
 
     most = pl.ds(0, 16 * (ROWS - 1))
-    peers_c = [(col + d) % COLS for d in range(COLS)]
     col_order = (4, 5, 3, 2, 6, 7, 1)
 
     def col_send(b, h):
@@ -275,8 +272,8 @@
     loads[8].wait()
     loads[9].wait()
     w_map[...] = dot(select_v[...], w_spec_v[...]).astype(BF16)
+    gates(1)
     forward(1)
-    gates(1)
     wait_bytes(w_out_v.at[pl.ds(0, 256), pl.ds(0, OUT)], rwo)
     for d in range(1, 4):
         share_out(quarter, 2, swy, rwy, (row // 4 * 4 + (row % 4 + d) % 4, col)).start()
@@ -328,7 +325,7 @@
         pltpu.VMEM((CHANNELS, D), BF16),
         pltpu.VMEM((CHANNELS, D), BF16),
         pltpu.VMEM((D, D), BF16),
-        pltpu.VMEM((2 * WIDTH, WIDTH), BF16),
+        pltpu.VMEM((WIDTH, 2 * WIDTH), BF16),
         pltpu.VMEM((2, 512, 512), BF16),
         pltpu.VMEM((2, 256, 256), F32),
         pltpu.VMEM((256, 512), BF16),

time: 49.2 us -> 47.4 us (0.963)
  Pallas kernels: 48.1 us -> 46.3 us
    pallas_call x1, Pallas kernels: 48.1 us -> 46.3 us  [on_device(): pl.pallas_call(kernel, out_shape=pltpu.VMEM((SEQS, LOCAL, OUT), BF16), in...]
where the time goes in v5:
time: 47.4 us; the launch traced here: 47.3 us
  Pallas kernels  46.3 us (98%)
  local copies, waits for them, and re-layouts  0.97 us (2%)
    pallas_call x1, Pallas kernels, on_device(): pl.pallas_call(kernel, out_shape=pltpu.VMEM((SEQS, LOCAL, OUT), BF16), in...  46.3 us
    unnamed x1, local copies, waits for them, and re-layouts  0.97 us

profile of v5, /device:TPU:1, one launch (start us, length us, event | category | flops | bytes accessed | tf_op | source)
XLA Modules:
  0.0 47.3 jit_solution(12503572065545535618)
XLA Ops:
  0.0 46.3 %fourier_mix.1 = bf16[2,2048,128]{2,1,0:T(8,128)(2,1)S(1)} custom-call(bf16[2,2048,1024]{2,1,0:T(8,128)(2,1)} %tokens.1, f32[1,1024]{1,0:T(1,128)} %bitcast.3, bf16[64,1024]{1,0:T(8,128)(2,1)} %bitcast.2, bf16[1024,1024]{1,0:T(8,128)(2,1)} %w_gate.1, bf16[512,1024]{1,0:T(8,128)(2,1)} %w_spec.1, bf16[1024,128]{1,0:T(8,128)(2,1)} %w_out.1, ...), custom_call_target="tpu_custom_call" | custom-call | tf_op jit(solution)/shard_map/fourier_mix/pallas_call | solution.py:350
  46.3 1.0 %copy.13 = bf16[2,2048,128]{2,1,0:T(8,128)(2,1)} copy(bf16[2,2048,128]{2,1,0:T(8,128)(2,1)S(1)} %fourier_mix.1) | data formatting | bytes 2097152

commit v6 on v5

--- a/solution.py
+++ b/solution.py
@@ -48,7 +48,7 @@
     for r in range(ROWS):
         for ch in range(2):
             for c in range(COLS):
-                select[r * 16 + ch * 8 + c, c * WIDTH + partner_channel(r, ch)] = 1.0
+                select[ch * 256 + r * 8 + c, c * WIDTH + partner_channel(r, ch)] = 1.0
     return (
         jnp.asarray(analysis.T, BF16),
         jnp.asarray(first, BF16),
@@ -103,6 +103,11 @@
         ((dz, dy) for dz in range(8) for dy in range(4) if dz or dy),
         key=lambda o: -(min(o[0], 8 - o[0]) + min(o[1], 4 - o[1])),
     )
+    paired = []
+    for dz, dy in far_first:
+        for one in ((dz, dy), (-dz % 8, -dy % 4)):
+            if one not in paired:
+                paired.append(one)
 
     barrier = pltpu.get_barrier_semaphore()
     for dz, dy in far_first:
@@ -154,15 +159,15 @@
 
         lax.fori_loop(0, ROWS // 8, pick, 0)
 
-    def row_send(src, dst, ssem, rsem):
-        mine = rows16(row)
-        for dz, dy in far_first:
+    def row_send(src, dst, ssem, rsem, block):
+        mine = block(row)
+        for dz, dy in paired:
             peer = peers_z[dz] + peers_y[dy]
             pltpu.make_async_remote_copy(
-                src_ref=src.at[rows16(peer)], dst_ref=dst.at[mine],
+                src_ref=src.at[block(peer)], dst_ref=dst.at[mine],
                 send_sem=ssem, recv_sem=rsem, device_id=(peer, col), device_id_type=MESH,
             ).start()
-        dst[mine, :] = src[mine, :]
+        dst[mine] = src[mine]
 
     def wait_bytes(ref, sem):
         pltpu.make_async_copy(ref, ref, sem).wait()
@@ -204,13 +209,17 @@
         for c in range(COLS):
             wide[h, c * WIDTH : (c + 1) * WIDTH, :] = recvx[b, h, c].astype(F32)
 
+        left = lax.broadcasted_iota(jnp.int32, (COLS, 128), 1) < 64
+
         def pick(i, _):
-            for u in range(4):
-                r = 4 * i + u
-                send2[b, h, rows16(r), :] = strided(wide, h, r, ROWS + r, COLS, WIDTH)
+            for u in range(16):
+                r = 16 * i + u
+                lo, hi = wide[h, pl.ds(r, COLS, WIDTH), :], wide[h, pl.ds(ROWS + r, COLS, WIDTH), :]
+                send2[b, 2 * h, r] = jnp.where(left, lo, pltpu.roll(hi, 64, 1)).astype(BF16)
+                send2[b, 2 * h + 1, r] = jnp.where(left, pltpu.roll(lo, 64, 1), hi).astype(BF16)
             return 0
 
-        lax.fori_loop(0, ROWS // 4, pick, 0)
+        lax.fori_loop(0, ROWS // 16, pick, 0)
 
     def gates(b):
         t = tok[b, col].astype(F32)
@@ -235,28 +244,31 @@
     every = pl.ds(0, D)
     other_core = (row, chip * 2 + 1 - core)
 
-    def finish(b, h):
-        lanes = pl.ds(128 * h, 128)
-        pre = dot(recv2[b, h], w_map[...], ((0,), (0,))).astype(BF16).astype(F32)
-        mixed = (sig[b, lanes] * pre).astype(BF16)
-        result[b, lanes] = dot(mixed, w_out_v[...]).astype(BF16)
-        place = pl.ds(pl.multiple_of(col * TILE + 128 * h, 128), 128)
+    def finish(b, t):
+        wait_bytes(recv2.at[b, t, pl.ds(0, ROWS - 1)], r2.at[b, t])
+        part = pl.ds(64 * t, 64)
+        block = jnp.transpose(recv2[b, t].astype(F32).reshape(COLS * ROWS, 128)).astype(BF16)
+        pre = dot(block[:64], w_map[:256]) + dot(block[64:], w_map[256:])
+        mixed = (sig[b, part] * pre.astype(BF16).astype(F32)).astype(BF16)
+        result[b, part] = dot(mixed, w_out_v[...]).astype(BF16)
+        place = pl.ds(pl.multiple_of(col * TILE + 64 * t, 64), 64)
 
         for d in col_order:
             peer = peers_c[d]
             pltpu.make_async_remote_copy(
-                src_ref=result.at[b, lanes, cols_of(peer)], dst_ref=out.at[b, place],
-                send_sem=so.at[b, h], recv_sem=ro.at[b, h], device_id=(row, peer), device_id_type=MESH,
+                src_ref=result.at[b, part, cols_of(peer)], dst_ref=out.at[b, place],
+                send_sem=so.at[b, t], recv_sem=ro.at[b, t], device_id=(row, peer), device_id_type=MESH,
             ).start()
-        pltpu.make_async_copy(result.at[b, lanes, cols_of(col)], out.at[b, place], own_o.at[b, h]).start()
+        pltpu.make_async_copy(result.at[b, part, cols_of(col)], out.at[b, place], own_o.at[b, t]).start()
 
     def forward(b):
-        row_send(send1.at[b], recv1.at[b], s1.at[b], r1.at[b])
+        row_send(send1.at[b], recv1.at[b], s1.at[b], r1.at[b], rows16)
 
     def back(b, h):
         wait_bytes(recvx.at[b, h, pl.ds(0, COLS - 1)], rx.at[b, h])
         regroup(b, h)
-        row_send(send2.at[b, h], recv2.at[b, h], s2.at[b, h], r2.at[b, h])
+        for t in (2 * h, 2 * h + 1):
+            row_send(send2.at[b, t], recv2.at[b, t], s2.at[b, t], r2.at[b, t], lambda r: r)
 
     project(0)
     pl.semaphore_wait(barrier, ROWS - 1 + COLS - 1)
@@ -283,20 +295,19 @@
     wait_bytes(recv1.at[0, most], r1.at[0])
     fourier(0)
     back(0, 0)
-    back(0, 1)
     wait_bytes(recv1.at[1, most], r1.at[1])
     fourier(1)
+    back(0, 1)
     wait_bytes(w_out_v.at[:, pl.ds(0, 2 * OUT)], rwn)
     wait_bytes(w_out_v.at[pl.ds(0, 768), pl.ds(0, OUT)], rwy)
     for d in range(1, 4):
         share_out(every, d, sf, rf, other_core).start()
+    wait_bytes(w_out_v.at[:, pl.ds(0, 4 * OUT)], rf)
     back(1, 0)
+    finish(0, 0)
     back(1, 1)
-    wait_bytes(w_out_v.at[:, pl.ds(0, 4 * OUT)], rf)
-    for b in range(SEQS):
-        for h in range(2):
-            wait_bytes(recv2.at[b, h, most], r2.at[b, h])
-            finish(b, h)
+    for b, t in ((0, 1), (0, 2), (0, 3), (1, 0), (1, 1), (1, 2), (1, 3)):
+        finish(b, t)
 
     wait_bytes(w_out_v.at[pl.ds(0, 256), pl.ds(0, OUT)], swo)
     wait_bytes(w_out_v.at[:, pl.ds(0, 2 * OUT)], swn)
@@ -305,17 +316,18 @@
     for b in range(SEQS):
         wait_bytes(send1.at[b, most], s1.at[b])
         for h in range(2):
-            lanes = pl.ds(128 * h, 128)
             wait_bytes(sendx.at[b, h, pl.ds(0, COLS - 1)], sx.at[b, h])
-            wait_bytes(send2.at[b, h, most], s2.at[b, h])
-            wait_bytes(result.at[b, lanes, pl.ds(0, (COLS - 1) * OUT)], so.at[b, h])
-            wait_bytes(out.at[b, pl.ds(0, (COLS - 1) * 128)], ro.at[b, h])
-            wait_bytes(result.at[b, lanes, pl.ds(0, OUT)], own_o.at[b, h])
+        for t in range(4):
+            part = pl.ds(64 * t, 64)
+            wait_bytes(send2.at[b, t, pl.ds(0, ROWS - 1)], s2.at[b, t])
+            wait_bytes(result.at[b, part, pl.ds(0, (COLS - 1) * OUT)], so.at[b, t])
+            wait_bytes(out.at[b, pl.ds(0, (COLS - 1) * 64)], ro.at[b, t])
+            wait_bytes(result.at[b, part, pl.ds(0, OUT)], own_o.at[b, t])
 
 
 def on_device(tokens, norm_gain, w_fourier_in, w_gate, w_spectrum, w_output):
     dma = pltpu.SemaphoreType.DMA
-    pair, halves = dma((SEQS,)), dma((SEQS, 2))
+    pair, halves, quarters = dma((SEQS,)), dma((SEQS, 2)), dma((SEQS, 4))
     scratch = [
         pltpu.VMEM((SEQS, TILES, TILE, D), BF16),
         pltpu.VMEM((1, D), F32),
@@ -338,12 +350,12 @@
         pltpu.VMEM((SEQS, 2, COLS, WIDTH, 128), BF16),
         pltpu.VMEM((SEQS, 2, COLS, WIDTH, 128), BF16),
         pltpu.VMEM((2, COLS * WIDTH, 128), F32),
-        pltpu.VMEM((SEQS, 2, 16 * ROWS, 128), BF16),
-        pltpu.VMEM((SEQS, 2, 16 * ROWS, 128), BF16),
+        pltpu.VMEM((SEQS, 4, ROWS, 8, 128), BF16),
+        pltpu.VMEM((SEQS, 4, ROWS, 8, 128), BF16),
         pltpu.VMEM((SEQS, TILE, D), F32),
         pltpu.VMEM((SEQS, TILE, D), BF16),
         dma((SEQS, TILES)), dma((10,)),
-        pair, pair, halves, halves, halves, halves, halves, halves, halves,
+        pair, pair, halves, halves, quarters, quarters, quarters, quarters, quarters,
         dma, dma, dma, dma, dma, dma, dma, dma,
     ]
     anywhere = pl.BlockSpec(memory_space=pl.ANY)

time: 47.4 us -> 47 us (level)
  no operation moved by 1% of the time
where the time goes in v6:
time: 47 us; the launch traced here: 46.8 us
  Pallas kernels  45.9 us (98%)
  local copies, waits for them, and re-layouts  0.97 us (2%)
    pallas_call x1, Pallas kernels, on_device(): pl.pallas_call(kernel, out_shape=pltpu.VMEM((SEQS, LOCAL, OUT), BF16), in...  45.9 us
    unnamed x1, local copies, waits for them, and re-layouts  0.97 us

profile of v6, /device:TPU:1, one launch (start us, length us, event | category | flops | bytes accessed | tf_op | source)
XLA Modules:
  0.0 46.8 jit_solution(7050100223600448882)
XLA Ops:
  0.0 45.9 %fourier_mix.1 = bf16[2,2048,128]{2,1,0:T(8,128)(2,1)S(1)} custom-call(bf16[2,2048,1024]{2,1,0:T(8,128)(2,1)} %tokens.1, f32[1,1024]{1,0:T(1,128)} %bitcast.3, bf16[64,1024]{1,0:T(8,128)(2,1)} %bitcast.2, bf16[1024,1024]{1,0:T(8,128)(2,1)} %w_gate.1, bf16[512,1024]{1,0:T(8,128)(2,1)} %w_spec.1, bf16[1024,128]{1,0:T(8,128)(2,1)} %w_out.1, ...), custom_call_target="tpu_custom_call" | custom-call | tf_op jit(solution)/shard_map/fourier_mix/pallas_call | solution.py:362
  45.9 1.0 %copy.13 = bf16[2,2048,128]{2,1,0:T(8,128)(2,1)} copy(bf16[2,2048,128]{2,1,0:T(8,128)(2,1)S(1)} %fourier_mix.1) | data formatting | bytes 2097152

commit v7 on v6

--- a/solution.py
+++ b/solution.py
@@ -247,7 +247,7 @@
     def finish(b, t):
         wait_bytes(recv2.at[b, t, pl.ds(0, ROWS - 1)], r2.at[b, t])
         part = pl.ds(64 * t, 64)
-        block = jnp.transpose(recv2[b, t].astype(F32).reshape(COLS * ROWS, 128)).astype(BF16)
+        block = jnp.transpose(recv2[b, t].reshape(COLS * ROWS, 128))
         pre = dot(block[:64], w_map[:256]) + dot(block[64:], w_map[256:])
         mixed = (sig[b, part] * pre.astype(BF16).astype(F32)).astype(BF16)
         result[b, part] = dot(mixed, w_out_v[...]).astype(BF16)

time: 47 us -> 46.9 us (level)
  no operation moved by 1% of the time
where the time goes in v7:
time: 46.9 us; the launch traced here: 46.8 us
  Pallas kernels  45.8 us (98%)
  local copies, waits for them, and re-layouts  0.97 us (2%)
    pallas_call x1, Pallas kernels, on_device(): pl.pallas_call(kernel, out_shape=pltpu.VMEM((SEQS, LOCAL, OUT), BF16), in...  45.8 us
    unnamed x1, local copies, waits for them, and re-layouts  0.97 us

profile of v7, /device:TPU:1, one launch (start us, length us, event | category | flops | bytes accessed | tf_op | source)
XLA Modules:
  0.0 46.8 jit_solution(6680004729439137826)
XLA Ops:
  0.0 45.8 %fourier_mix.1 = bf16[2,2048,128]{2,1,0:T(8,128)(2,1)S(1)} custom-call(bf16[2,2048,1024]{2,1,0:T(8,128)(2,1)} %tokens.1, f32[1,1024]{1,0:T(1,128)} %bitcast.3, bf16[64,1024]{1,0:T(8,128)(2,1)} %bitcast.2, bf16[1024,1024]{1,0:T(8,128)(2,1)} %w_gate.1, bf16[512,1024]{1,0:T(8,128)(2,1)} %w_spec.1, bf16[1024,128]{1,0:T(8,128)(2,1)} %w_out.1, ...), custom_call_target="tpu_custom_call" | custom-call | tf_op jit(solution)/shard_map/fourier_mix/pallas_call | solution.py:362
  45.8 1.0 %copy.13 = bf16[2,2048,128]{2,1,0:T(8,128)(2,1)} copy(bf16[2,2048,128]{2,1,0:T(8,128)(2,1)S(1)} %fourier_mix.1) | data formatting | bytes 2097152

commit v8 on v7

--- a/solution.py
+++ b/solution.py
@@ -302,8 +302,8 @@
     wait_bytes(w_out_v.at[pl.ds(0, 768), pl.ds(0, OUT)], rwy)
     for d in range(1, 4):
         share_out(every, d, sf, rf, other_core).start()
+    back(1, 0)
     wait_bytes(w_out_v.at[:, pl.ds(0, 4 * OUT)], rf)
-    back(1, 0)
     finish(0, 0)
     back(1, 1)
     for b, t in ((0, 1), (0, 2), (0, 3), (1, 0), (1, 1), (1, 2), (1, 3)):

time: 46.9 us -> 46.9 us (level)
  no operation moved by 1% of the time
where the time goes in v8:
time: 46.9 us; the launch traced here: 46.8 us
  Pallas kernels  45.8 us (98%)
  local copies, waits for them, and re-layouts  0.97 us (2%)
    pallas_call x1, Pallas kernels, on_device(): pl.pallas_call(kernel, out_shape=pltpu.VMEM((SEQS, LOCAL, OUT), BF16), in...  45.8 us
    unnamed x1, local copies, waits for them, and re-layouts  0.97 us

profile of v8, /device:TPU:1, one launch (start us, length us, event | category | flops | bytes accessed | tf_op | source)
XLA Modules:
  0.0 46.8 jit_solution(686637840297194991)
XLA Ops:
  0.0 45.8 %fourier_mix.1 = bf16[2,2048,128]{2,1,0:T(8,128)(2,1)S(1)} custom-call(bf16[2,2048,1024]{2,1,0:T(8,128)(2,1)} %tokens.1, f32[1,1024]{1,0:T(1,128)} %bitcast.3, bf16[64,1024]{1,0:T(8,128)(2,1)} %bitcast.2, bf16[1024,1024]{1,0:T(8,128)(2,1)} %w_gate.1, bf16[512,1024]{1,0:T(8,128)(2,1)} %w_spec.1, bf16[1024,128]{1,0:T(8,128)(2,1)} %w_out.1, ...), custom_call_target="tpu_custom_call" | custom-call | tf_op jit(solution)/shard_map/fourier_mix/pallas_call | solution.py:362
  45.8 1.0 %copy.13 = bf16[2,2048,128]{2,1,0:T(8,128)(2,1)} copy(bf16[2,2048,128]{2,1,0:T(8,128)(2,1)S(1)} %fourier_mix.1) | data formatting | bytes 2097152

commit v9 on v8

--- a/solution.py
+++ b/solution.py
@@ -305,8 +305,9 @@
     back(1, 0)
     wait_bytes(w_out_v.at[:, pl.ds(0, 4 * OUT)], rf)
     finish(0, 0)
+    finish(0, 1)
     back(1, 1)
-    for b, t in ((0, 1), (0, 2), (0, 3), (1, 0), (1, 1), (1, 2), (1, 3)):
+    for b, t in ((0, 2), (0, 3), (1, 0), (1, 1), (1, 2), (1, 3)):
         finish(b, t)
 
     wait_bytes(w_out_v.at[pl.ds(0, 256), pl.ds(0, OUT)], swo)

time: 46.9 us -> 46.9 us (level)
  no operation moved by 1% of the time
where the time goes in v9:
time: 46.9 us; the launch traced here: 46.7 us
  Pallas kernels  45.8 us (98%)
  local copies, waits for them, and re-layouts  0.97 us (2%)
    pallas_call x1, Pallas kernels, on_device(): pl.pallas_call(kernel, out_shape=pltpu.VMEM((SEQS, LOCAL, OUT), BF16), in...  45.8 us
    unnamed x1, local copies, waits for them, and re-layouts  0.97 us

profile of v9, /device:TPU:1, one launch (start us, length us, event | category | flops | bytes accessed | tf_op | source)
XLA Modules:
  0.0 46.7 jit_solution(6272536449998484690)
XLA Ops:
  0.0 45.8 %fourier_mix.1 = bf16[2,2048,128]{2,1,0:T(8,128)(2,1)S(1)} custom-call(bf16[2,2048,1024]{2,1,0:T(8,128)(2,1)} %tokens.1, f32[1,1024]{1,0:T(1,128)} %bitcast.3, bf16[64,1024]{1,0:T(8,128)(2,1)} %bitcast.2, bf16[1024,1024]{1,0:T(8,128)(2,1)} %w_gate.1, bf16[512,1024]{1,0:T(8,128)(2,1)} %w_spec.1, bf16[1024,128]{1,0:T(8,128)(2,1)} %w_out.1, ...), custom_call_target="tpu_custom_call" | custom-call | tf_op jit(solution)/shard_map/fourier_mix/pallas_call | solution.py:363
  45.8 1.0 %copy.13 = bf16[2,2048,128]{2,1,0:T(8,128)(2,1)} copy(bf16[2,2048,128]{2,1,0:T(8,128)(2,1)S(1)} %fourier_mix.1) | data formatting | bytes 2097152
